TPU v7x, 768 devices: a whole 4x8x12 slice. The times are simulated.
768 devices in a mesh: fs: 96 (over z, y), tp: 8 (over x, core).
Axes of the slice: x: 4, y: 8, z: 12, core: 2. Of those that a mesh axis runs over, the one named last changes fastest.
Arguments:
- stream_in: bfloat16 [24576, 2112], P('fs'), may hold values from -6 to 6
- norm_gains: float32 [6, 2112], replicated, may hold values from 0.1 to 1.9
- gate_proj: bfloat16 [2112, 3072], P('fs', 'tp'), may hold values from -0.125 to 0.125
- up_proj: bfloat16 [2112, 3072], P('fs', 'tp'), may hold values from -0.125 to 0.125
- down_proj: bfloat16 [2112, 3072], P('fs', 'tp'), may hold values from -0.109375 to 0.109375
- outer_gate: bfloat16 [2112, 1056], P('fs', 'tp'), may hold values from -0.125 to 0.125
- inner_gate: bfloat16 [2112, 1056], P('fs', 'tp'), may hold values from -0.125 to 0.125
- value_proj: bfloat16 [2112, 1056], P('fs', 'tp'), may hold values from -0.125 to 0.125
- mixer_out: bfloat16 [2112, 1056], P('fs', 'tp'), may hold values from -0.1875 to 0.1875
- conv_taps: bfloat16 [3, 1056], replicated, may hold values from -3 to 3
Outputs:
- stream_out: bfloat16 [24576, 2112], P('fs')
All inputs are finite; a program needn't handle non-finite values.
Results may differ from a plain program's by a relative error of at most 0.02.
Values may be sent and summed in bfloat16 or wider, within the bound.
A program may use at most 64 MiB of HBM per device.

v0:
```python
import jax
import jax.numpy as jnp
from jax import lax
from jax.sharding import PartitionSpec as P

CONV_K = 3


EPSILON = 1e-06


def in_blocks(shard, dim, devices):
    shape = shard.shape
    tiles = shard.reshape(*shape[:dim], devices, shape[dim] // devices, *shape[dim + 1 :])
    return jnp.moveaxis(tiles, dim, 0)


def summed_on_arrival(shard, axis, dim):
    devices = lax.axis_size(axis)
    tiles = lax.all_to_all(in_blocks(shard, dim, devices), axis, 0, 0, tiled=True)
    return jnp.sum(tiles.astype(jnp.float32), axis=0)


def copy_for_each(shard, axis):
    devices = lax.axis_size(axis)
    return lax.all_to_all(
        jnp.broadcast_to(shard[None], (devices, *shard.shape)), axis, 0, 0, tiled=True
    )


def of_everyone(shard, axis):
    return copy_for_each(shard, axis).sum(axis=0)


def in_order(tiles, dim):
    shape = list(tiles.shape[1:])
    shape[dim] *= tiles.shape[0]
    return jnp.moveaxis(tiles, 0, dim).reshape(shape)


def gather_directly(shard, axis, dim):
    return in_order(copy_for_each(shard, axis), dim)


def in_one_piece(arrays, axis, dim, along):
    both = jnp.concatenate(arrays, axis=along)
    result, at, gathered = (lax.all_gather(both, axis, axis=dim, tiled=True), 0, [])
    for a in arrays:
        gathered.append(lax.slice_in_dim(result, at, at + a.shape[along], axis=along))
        at += a.shape[along]
    return tuple(gathered)


def scaled(values, gain):
    return values * lax.rsqrt(jnp.mean(values * values, axis=-1, keepdims=True) + EPSILON) * gain


def narrow(inner, weight, stream, gain, factor):
    partial_value = lax.dot_general(
        inner, weight, (((1,), (1,)), ((), ())), preferred_element_type=jnp.float32
    )
    share = summed_on_arrival(partial_value.astype(jnp.bfloat16), "tp", 1)
    width = share.shape[1]
    start = lax.axis_index("tp") * width
    total_width = width * lax.axis_size("tp")
    stream_share = lax.dynamic_slice_in_dim(stream, start, width, 1).astype(jnp.float32)
    gain_share = lax.dynamic_slice_in_dim(gain, start, width, 0)
    squares = of_everyone(jnp.sum(share * share, axis=-1), "tp")
    normed = share * lax.rsqrt(squares / total_width + EPSILON)[:, None] * gain_share
    result_share = (stream_share + factor * normed).astype(jnp.bfloat16)
    return gather_directly(result_share, "tp", 1)


def half_step(stream, weights, pre_gain, post_gain):
    gate_full, up_full, down_full = weights
    normed = scaled(stream.astype(jnp.float32), pre_gain).astype(jnp.bfloat16)
    gate = jnp.dot(normed, gate_full, preferred_element_type=jnp.float32)
    upward = jnp.dot(normed, up_full, preferred_element_type=jnp.float32)
    hidden = (jax.nn.silu(gate) * upward).astype(jnp.bfloat16)
    return narrow(hidden, down_full, stream, post_gain, 0.5)


def mixer_step(stream, weights, conv_taps, pre_gain, post_gain):
    outer_full, inner_full, value_full, out_full = weights
    channels = outer_full.shape[1]
    normed = scaled(stream.astype(jnp.float32), pre_gain).astype(jnp.bfloat16)
    outer = (
        jnp.dot(normed, outer_full, preferred_element_type=jnp.float32)
        .astype(jnp.bfloat16)
        .astype(jnp.float32)
    )
    inner = (
        jnp.dot(normed, inner_full, preferred_element_type=jnp.float32)
        .astype(jnp.bfloat16)
        .astype(jnp.float32)
    )
    value = (
        jnp.dot(normed, value_full, preferred_element_type=jnp.float32)
        .astype(jnp.bfloat16)
        .astype(jnp.float32)
    )
    gated = inner * value
    taps = lax.dynamic_slice_in_dim(conv_taps, lax.axis_index("tp") * channels, channels, 1).astype(
        jnp.float32
    )
    length = gated.shape[0]
    padded = jnp.concatenate([jnp.zeros((CONV_K - 1, channels), jnp.float32), gated], axis=0)
    conv = jnp.zeros_like(gated)
    for offset in range(CONV_K):
        conv = conv + taps[offset] * padded[offset : offset + length]
    mixed = (outer * conv).astype(jnp.bfloat16)
    return narrow(mixed, out_full, stream, post_gain, 1.0)


def local(
    stream_in,
    norm_gains,
    gate_proj,
    up_proj,
    down_proj,
    outer_gate,
    inner_gate,
    value_proj,
    mixer_out,
    conv_taps,
):
    gathered = in_one_piece(
        (gate_proj, up_proj, down_proj, outer_gate, inner_gate, value_proj, mixer_out), "fs", 0, 1
    )
    mlp_full = gathered[:3]
    mixer_full = gathered[3:]
    stream = half_step(stream_in, mlp_full, norm_gains[0], norm_gains[1])
    stream = mixer_step(stream, mixer_full, conv_taps, norm_gains[2], norm_gains[3])
    return half_step(stream, mlp_full, norm_gains[4], norm_gains[5])


def solution(mesh):
    return jax.shard_map(
        local,
        mesh=mesh,
        in_specs=(
            P("fs", None),
            P(),
            P("fs", "tp"),
            P("fs", "tp"),
            P("fs", "tp"),
            P("fs", "tp"),
            P("fs", "tp"),
            P("fs", "tp"),
            P("fs", "tp"),
            P(),
        ),
        out_specs=P("fs", None),
        check_vma=False,
    )
```

profile of v0, /device:TPU:1, one launch (start us, length us, event | category | flops | bytes accessed | tf_op | source)
XLA Modules:
  0.0 340.6 jit_solution(16837940732896271139)
XLA Ops:
  6.5 1.5 concatenate.6
  8.1 1.6 fusion
  10.9 137.5 %all-gather.3.cloned.1.call-done = bf16[96,22,1680]{2,1,0:T(8,128)(2,1)} async-done(((bf16[1,22,1680]{2,1,0:T(8,128)(2,1)}), bf16[96,22,1680]{2,1,0:T(8,128)(2,1)}) %all-gather.3.cloned.1.call-update) | async-done | bytes 7096336 | tf_op jit(solution)/shard_map/all_gather | solution.py:47
  148.4 11.4 %reshape.91 = bf16[2112,1680]{1,0:T(8,128)(2,1)} reshape(bf16[96,22,1680]{2,1,0:T(8,128)(2,1)} %all-gather.3.cloned.1.call-done) | data formatting | bytes 14192640
  159.8 3.0 fusion.11
  162.7 4.1 %convolution_convert_fusion.1 = bf16[256,2112]{0,1:T(8,128)(2,1)S(1)} fusion(bf16[2112,1680]{1,0:T(8,128)(2,1)} %reshape.91, f32[256,384]{1,0:T(8,128)S(1)} %fusion.11, bf16[256,2112]{0,1:T(8,128)(2,1)S(1)} %copy-done, f32[2112]{0:T(1024)S(1)} %get-tuple-element.11, f32[256]{0:T(256)S(1)} %add_rsqrt_fusion.5), kind=kOutput, calls=%fused_computation.1 | convolution fusion | flops 833765376 | bytes 5809408 | tf_op jit(solution)/shard_map/dot_general | solution.py:59
  166.9 25.7 %all_to_all.48 = bf16[8,256,264]{1,2,0:T(8,128)(2,1)S(1)} all-to-all(bf16[8,256,264]{1,2,0:T(8,128)(2,1)S(1)} %bitcast.35), channel_id=1, replica_groups=mesh['fs'=96,'tp'=8] {'tp'}, dimensions={0} | all-to-all | bytes 2162688 | tf_op jit(solution)/shard_map/all_to_all | solution.py:20
  193.4 3.8 %all-to-all-start.1 = ((f32[8,1,256]{2,1,0:T(1,128)}), f32[8,1,256]{2,1,0:T(1,128)S(1)}, u32[]{:S(2)}, u32[]{:S(2)}) async-start(f32[8,1,256]{2,1,0:T(1,128)} %broadcast_in_dim.12), calls=%async_computation.1 | async-start | bytes 16384 | tf_op jit(solution)/shard_map/all_to_all | solution.py:26
  197.3 4.5 %all-to-all-done.1 = f32[8,1,256]{2,1,0:T(1,128)S(1)} async-done(((f32[8,1,256]{2,1,0:T(1,128)}), f32[8,1,256]{2,1,0:T(1,128)S(1)}, u32[]{:S(2)}, u32[]{:S(2)}) %all-to-all-start.1) | async-done | bytes 8224 | tf_op jit(solution)/shard_map/all_to_all | solution.py:26
  203.0 4.2 %all-to-all-start.2 = ((bf16[8,256,264]{1,2,0:T(8,128)(2,1)}), bf16[8,256,264]{1,2,0:T(8,128)(2,1)S(1)}, u32[]{:S(2)}, u32[]{:S(2)}) async-start(bf16[8,256,264]{1,2,0:T(8,128)(2,1)} %broadcast_in_dim.13), calls=%async_computation.2 | async-start | bytes 2162688 | tf_op jit(solution)/shard_map/all_to_all | solution.py:26
  207.9 14.6 %all-to-all-done.2 = bf16[8,256,264]{1,2,0:T(8,128)(2,1)S(1)} async-done(((bf16[8,256,264]{1,2,0:T(8,128)(2,1)}), bf16[8,256,264]{1,2,0:T(8,128)(2,1)S(1)}, u32[]{:S(2)}, u32[]{:S(2)}) %all-to-all-start.2) | async-done | bytes 1081376 | tf_op jit(solution)/shard_map/all_to_all | solution.py:26
  223.2 2.5 fusion.31
  225.7 2.5 fusion.30
  228.2 2.7 convolution_convert_fusion.2
  230.8 19.1 %all_to_all.49 = bf16[8,256,264]{1,2,0:T(8,128)(2,1)S(1)} all-to-all(bf16[8,256,264]{1,2,0:T(8,128)(2,1)S(1)} %bitcast.33), channel_id=1, replica_groups=mesh['fs'=96,'tp'=8] {'tp'}, dimensions={0} | all-to-all | bytes 2162688 | tf_op jit(solution)/shard_map/all_to_all | solution.py:20
  250.8 3.8 %all-to-all-start.4 = ((f32[8,1,256]{2,1,0:T(1,128)}), f32[8,1,256]{2,1,0:T(1,128)S(1)}, u32[]{:S(2)}, u32[]{:S(2)}) async-start(f32[8,1,256]{2,1,0:T(1,128)} %broadcast_in_dim.14), calls=%async_computation.4 | async-start | bytes 16384 | tf_op jit(solution)/shard_map/all_to_all | solution.py:26
  254.7 4.5 %all-to-all-done.4 = f32[8,1,256]{2,1,0:T(1,128)S(1)} async-done(((f32[8,1,256]{2,1,0:T(1,128)}), f32[8,1,256]{2,1,0:T(1,128)S(1)}, u32[]{:S(2)}, u32[]{:S(2)}) %all-to-all-start.4) | async-done | bytes 8224 | tf_op jit(solution)/shard_map/all_to_all | solution.py:26
  259.4 18.8 %all_to_all.50 = bf16[8,256,264]{1,2,0:T(8,128)(2,1)S(1)} all-to-all(bf16[8,256,264]{1,2,0:T(8,128)(2,1)S(1)} %broadcast_in_dim.15), channel_id=1, replica_groups=mesh['fs'=96,'tp'=8] {'tp'}, dimensions={0} | all-to-all | bytes 2162688 | tf_op jit(solution)/shard_map/all_to_all | solution.py:26
  278.6 3.0 fusion.9
  281.6 4.1 %convolution_convert_fusion = bf16[256,2112]{0,1:T(8,128)(2,1)S(1)} fusion(bf16[2112,1680]{1,0:T(8,128)(2,1)} %reshape.91, f32[256,384]{1,0:T(8,128)S(1)} %fusion.9, bf16[256,2112]{0,1:T(8,128)(2,1)S(1)} %bitcast.30, f32[2112]{0:T(1024)S(1)} %get-tuple-element.13, f32[256]{0:T(256)S(1)} %add_rsqrt_fusion.1), kind=kOutput, calls=%fused_computation | convolution fusion | flops 833765376 | bytes 5809408 | tf_op jit(solution)/shard_map/dot_general | solution.py:59
  285.7 18.7 %all_to_all.51 = bf16[8,256,264]{1,2,0:T(8,128)(2,1)S(1)} all-to-all(bf16[8,256,264]{1,2,0:T(8,128)(2,1)S(1)} %bitcast.34), channel_id=1, replica_groups=mesh['fs'=96,'tp'=8] {'tp'}, dimensions={0} | all-to-all | bytes 2162688 | tf_op jit(solution)/shard_map/all_to_all | solution.py:20
  305.2 3.8 %all-to-all-start.7 = ((f32[8,1,256]{2,1,0:T(1,128)}), f32[8,1,256]{2,1,0:T(1,128)S(1)}, u32[]{:S(2)}, u32[]{:S(2)}) async-start(f32[8,1,256]{2,1,0:T(1,128)} %broadcast_in_dim.16), calls=%async_computation.7 | async-start | bytes 16384 | tf_op jit(solution)/shard_map/all_to_all | solution.py:26
  309.1 4.5 %all-to-all-done.7 = f32[8,1,256]{2,1,0:T(1,128)S(1)} async-done(((f32[8,1,256]{2,1,0:T(1,128)}), f32[8,1,256]{2,1,0:T(1,128)S(1)}, u32[]{:S(2)}, u32[]{:S(2)}) %all-to-all-start.7) | async-done | bytes 8224 | tf_op jit(solution)/shard_map/all_to_all | solution.py:26
  313.9 18.8 %all_to_all.52 = bf16[8,256,264]{1,2,0:T(8,128)(2,1)S(1)} all-to-all(bf16[8,256,264]{1,2,0:T(8,128)(2,1)S(1)} %broadcast_in_dim.17), channel_id=1, replica_groups=mesh['fs'=96,'tp'=8] {'tp'}, dimensions={0} | all-to-all | bytes 2162688 | tf_op jit(solution)/shard_map/all_to_all | solution.py:26
  (38 shorter events, 8.3 us)
Async XLA Ops:
  6.5 141.9 %all-gather.3.cloned.1.call-start = ((), (), s32[]{:S(2)}) async-start(), calls=%async_computation.9 | async-start | bytes 8343552 | tf_op jit(solution)/shard_map/all_gather | solution.py:47
  10.9 148.9 %copy-start = (bf16[256,2112]{0,1:T(8,128)(2,1)S(1)}, bf16[256,2112]{0,1:T(8,128)(2,1)}, u32[]{:S(2)}) copy-start(bf16[256,2112]{0,1:T(8,128)(2,1)} %param.10) | copy-start | bytes 3244036
  193.4 8.4 %all-to-all-start.1 = ((f32[8,1,256]{2,1,0:T(1,128)}), f32[8,1,256]{2,1,0:T(1,128)S(1)}, u32[]{:S(2)}, u32[]{:S(2)}) async-start(f32[8,1,256]{2,1,0:T(1,128)} %broadcast_in_dim.12), calls=%async_computation.1 | async-start | bytes 16384 | tf_op jit(solution)/shard_map/all_to_all | solution.py:26
  203.0 19.5 %all-to-all-start.2 = ((bf16[8,256,264]{1,2,0:T(8,128)(2,1)}), bf16[8,256,264]{1,2,0:T(8,128)(2,1)S(1)}, u32[]{:S(2)}, u32[]{:S(2)}) async-start(bf16[8,256,264]{1,2,0:T(8,128)(2,1)} %broadcast_in_dim.13), calls=%async_computation.2 | async-start | bytes 2162688 | tf_op jit(solution)/shard_map/all_to_all | solution.py:26
  250.8 8.4 %all-to-all-start.4 = ((f32[8,1,256]{2,1,0:T(1,128)}), f32[8,1,256]{2,1,0:T(1,128)S(1)}, u32[]{:S(2)}, u32[]{:S(2)}) async-start(f32[8,1,256]{2,1,0:T(1,128)} %broadcast_in_dim.14), calls=%async_computation.4 | async-start | bytes 16384 | tf_op jit(solution)/shard_map/all_to_all | solution.py:26
  305.2 8.4 %all-to-all-start.7 = ((f32[8,1,256]{2,1,0:T(1,128)}), f32[8,1,256]{2,1,0:T(1,128)S(1)}, u32[]{:S(2)}, u32[]{:S(2)}) async-start(f32[8,1,256]{2,1,0:T(1,128)} %broadcast_in_dim.16), calls=%async_computation.7 | async-start | bytes 16384 | tf_op jit(solution)/shard_map/all_to_all | solution.py:26
Sparse Core Ops, SparseCore 0:
  11.0 137.3 all-gather.2
where the time goes:
time: 342 us; the launch traced here: 341 us
  waiting for transfers between devices  166 us (49%)
  blocking collectives  101 us (30%)
  matrix products  21.8 us (6%)
  local copies, waits for them, and re-layouts  18.4 us (5%)
  starting transfers between devices  15.6 us (5%)
  between operations  13.5 us (4%)
  other arithmetic  4.36 us (1%)
    all_gather x1, waiting for transfers between devices, in_one_piece(): lax.all_gather(both, axis, axis=dim, tiled=True)  138 us
    all_to_all x3, blocking collectives, summed_on_arrival(): lax.all_to_all(in_blocks(shard, dim, devices), axis, 0, 0, tiled=True)  63.5 us
    all_to_all x2, blocking collectives, copy_for_each(): lax.all_to_all(jnp.broadcast_to(shard[None], (devices, *shard.shape)), ax...  37.7 us
    all_to_all x4, waiting for transfers between devices, copy_for_each(): lax.all_to_all(jnp.broadcast_to(shard[None], (devices, *shard.shape)), ax...  28.2 us
    all_to_all x4, starting transfers between devices, copy_for_each(): lax.all_to_all(jnp.broadcast_to(shard[None], (devices, *shard.shape)), ax...  15.6 us
    unnamed x4, local copies, waits for them, and re-layouts  12.4 us
    dot_general x3, matrix products, narrow(): lax.dot_general(inner, weight, (((1,), (1,)), ((), ())), preferred_elemen...  11 us
  transfers between devices with their start and end apart: 5, of which 5 were waited for; matrix products, arithmetic and copies ran while one was open for 1% of the time, Pallas kernels for 0%

commit v1 on v0

v1 whole, which is shorter than its diff:
```python
import jax
import jax.numpy as jnp
from jax import lax
from jax.experimental import pallas as pl
from jax.experimental.pallas import tpu as pltpu
from jax.sharding import PartitionSpec as P

EPSILON = 1e-06
NX, NY, NZ = 4, 8, 12
D = 2112
OWN = 22
PAD = 24
DP = 96 * PAD
QN, QW = 3, DP // 3
HALF, SHARE = 128, 32
HID, CH = 384, 132
CW_A, CW_B = 896, 896
F32, BF16 = jnp.float32, jnp.bfloat16


def windows():
    out = []
    for j in range(6):
        base = (352 * j) // 128 * 128
        out.append((j, base, min(512, D - base)))
    return out


def spread(j, base, width):
    row = lax.broadcasted_iota(jnp.int32, (width, 384), 0).astype(F32) + float(base)
    col = lax.broadcasted_iota(jnp.int32, (width, 384), 1).astype(F32)
    block = jnp.floor((col + 0.5) / float(PAD))
    inside = col - block * float(PAD)
    target = float(352 * j) + block * float(OWN) + inside
    hit = (row == target) & (inside < float(OWN) - 0.5)
    return jnp.where(hit, 1.0, 0.0).astype(BF16)


def dot(a, b):
    return lax.dot_general(a, b, (((1,), (0,)), ((), ())), preferred_element_type=F32)


def dot_t(a, b):
    return lax.dot_general(a, b, (((1,), (1,)), ((), ())), preferred_element_type=F32)


def kernel(
    wa_in, wb_in, stream, gains, taps, out,
    wa, wb, xs, xn, hid, part, got, tot, res, fin, acc, halo_out, halo_in,
    g_send, g_recv, p_send, p_recv, rs_send, rs_recv, ag_send, ag_recv,
    fo_send, fo_recv, fp_send, fp_recv, h_send, h_recv, l_sem,
):
    fs, tp = lax.axis_index("fs"), lax.axis_index("tp")
    z, y = fs // NY, fs % NY
    x, c = tp // 2, tp % 2
    s = 1 - 2 * c

    def at(zz, yy, xx, cc):
        return {"fs": zz * NY + yy, "tp": xx * 2 + cc}

    def ymod(v):
        return lax.rem(v + NY, NY)

    def zmod(v):
        return lax.rem(v + NZ, NZ)

    here = [wa.at[c, z, pl.ds(pl.multiple_of(y * PAD, 8), PAD), :], wb.at[c, z, pl.ds(pl.multiple_of(y * PAD, 8), PAD), :]]
    own = [pltpu.make_async_copy(src, dst, l_sem.at[i]) for i, (src, dst) in enumerate(zip((wa_in, wb_in), here))]
    for copy in own:
        copy.start()

    y_fwd, y_back = at(z, ymod(y + s), x, c), at(z, ymod(y - s), x, c)
    z_fwd, z_back = at(zmod(z + s), y, x, c), at(zmod(z - s), y, x, c)
    mate = at(z, y, x, 1 - c)
    peers = [at(z, y, lax.rem(x + d, NX), c) for d in (1, 2, 3)]
    barrier = pltpu.get_barrier_semaphore()
    for dev in [y_fwd, y_back, z_fwd, z_back, mate] + peers:
        pl.semaphore_signal(barrier, inc=1, device_id=dev, device_id_type=pl.DeviceIdType.MESH)
    pl.semaphore_wait(barrier, 8)
    for copy in own:
        copy.wait()

    ys = [y] + [ymod(y - s * d) for d in range(1, 5)] + [ymod(y + s * d) for d in range(1, 4)]
    zs = [z] + [zmod(z - s * d) for d in range(1, 7)] + [zmod(z + s * d) for d in range(1, 6)]
    bufs = (wa, wb)

    def remote(which, src_zz, src_yy, index, dev):
        ref = bufs[which].at[c, src_zz, pl.ds(pl.multiple_of(src_yy * PAD, 8), PAD), :]
        return pltpu.make_async_remote_copy(
            src_ref=ref, dst_ref=ref, send_sem=g_send.at[which, index], recv_sem=g_recv.at[which, index],
            device_id=dev, device_id_type=pl.DeviceIdType.MESH,
        )

    started = []

    def push(which, jz, jy, to_jz, to_jy, dev):
        copy = remote(which, zs[jz], ys[jy], to_jz * NY + to_jy, dev)
        copy.start()
        started.append(copy)

    def take(which, jz, jy):
        remote(which, zs[jz], ys[jy], jz * NY + jy, y_fwd).wait_recv()

    y_hops = ((0, 4, y_fwd), (4, 3, y_back))
    z_hops = ((0, 6, z_fwd), (6, 5, z_back))

    def y_next(which, jz, jy):
        for off, hops, dev in y_hops:
            if jy == 0:
                push(which, jz, 0, jz, off + 1, dev)
            elif off < jy < off + hops:
                push(which, jz, jy, jz, jy + 1, dev)

    def z_next(which, jz, jy):
        for off, hops, dev in z_hops:
            if jz == 0:
                push(which, 0, jy, off + 1, jy, dev)
            elif off < jz < off + hops:
                push(which, jz, jy, jz + 1, jy, dev)

    def y_far(jy):
        return jy if jy <= 4 else jy - 4

    def z_far(jz):
        return jz if jz <= 6 else jz - 6

    mates = []

    def to_mate(which, sub, index):
        ref = bufs[which].at[c, zs[index], pl.ds(0, NY * PAD), :] if which == 0 else sub
        copy = pltpu.make_async_remote_copy(
            src_ref=ref, dst_ref=ref, send_sem=p_send.at[which, index], recv_sem=p_recv.at[which, index],
            device_id=mate, device_id_type=pl.DeviceIdType.MESH,
        )
        copy.start()
        mates.append(copy)

    y_order = [0, 1, 5, 2, 6, 3, 7, 4]
    z_order = [0, 1, 7, 2, 8, 3, 9, 4, 10, 5, 11, 6]

    z_next(0, 0, 0)
    y_next(1, 0, 0)
    y_next(0, 0, 0)
    z_next(1, 0, 0)

    half = stream[pl.ds(pl.multiple_of(c * HALF, HALF), HALF), :]
    mine = stream[pl.ds(pl.multiple_of(c * HALF + x * SHARE, SHARE), SHARE), :]
    for j, base, width in windows():
        m = spread(j, base, width)
        xs[:, 384 * j:384 * (j + 1)] = dot(half[:, base:base + width], m).astype(BF16)
        res[:, 384 * j:384 * (j + 1)] = dot(mine[:, base:base + width], m).astype(BF16)
    wide = xs[...].astype(F32)
    scale = lax.rsqrt(jnp.sum(wide * wide, axis=-1, keepdims=True) / D + EPSILON)
    for q in range(QN):
        cols = slice(q * QW, (q + 1) * QW)
        xn[q] = (wide[:, cols] * scale * gains[0:1, cols]).astype(BF16)

    for slot in range(1, 11):
        for jy in y_order:
            if y_far(jy) == slot:
                take(0, 0, jy)
                z_next(0, 0, jy)
                y_next(0, 0, jy)
        for jz in z_order:
            if z_far(jz) == slot:
                take(1, jz, 0)
                y_next(1, jz, 0)
                z_next(1, jz, 0)
        for jz in z_order:
            for jy in y_order:
                if y_far(jy) + z_far(jz) == slot:
                    if jz > 0:
                        take(0, jz, jy)
                        z_next(0, jz, jy)
                    if jy > 0:
                        take(1, jz, jy)
                        y_next(1, jz, jy)
        for jz in range(NZ):
            if slot == 4 + z_far(jz):
                to_mate(0, None, jz)
        for jy in range(NY):
            if slot == 6 + y_far(jy):
                to_mate(1, wb.at[c, :, pl.ds(pl.multiple_of(ys[jy] * PAD, 8), PAD), :], jy)
    for copy in mates:
        copy.wait_recv()

    def weight(buf, w, q, lo, hi):
        return buf[w, 4 * q:4 * q + 4, 0:NY * PAD, lo:hi].reshape(QW, hi - lo)

    def project(buf, w, lo, hi):
        total = dot(xn[0], weight(buf, w, 0, lo, hi))
        for q in range(1, QN):
            total = total + dot(xn[q], weight(buf, w, q, lo, hi))
        return total

    def narrow(layer, parts, gain, factor, last):
        copies = []
        for q in range(QN):
            total = parts(q)
            part[layer, q] = total.astype(BF16)
            for d in (2, 1, 3):
                there = lax.rem(x + d, NX)
                copy = pltpu.make_async_remote_copy(
                    src_ref=part.at[layer, q, pl.ds(pl.multiple_of(there * SHARE, SHARE), SHARE), :],
                    dst_ref=got.at[d - 1, q],
                    send_sem=rs_send.at[layer, d - 1, q], recv_sem=rs_recv.at[layer, d - 1, q],
                    device_id=peers[d - 1], device_id_type=pl.DeviceIdType.MESH,
                )
                copy.start()
                copies.append((q, copy))
        squares = jnp.zeros((SHARE, 1), F32)
        for q in range(QN):
            for at_q, copy in copies:
                if at_q == q:
                    copy.wait_recv()
            total = part[layer, q, pl.ds(pl.multiple_of(x * SHARE, SHARE), SHARE), :].astype(F32)
            for d in range(3):
                total = total + got[d, q].astype(F32)
            tot[:, q * QW:(q + 1) * QW] = total
            squares = squares + jnp.sum(total * total, axis=-1, keepdims=True)
        scale = lax.rsqrt(squares / D + EPSILON)
        fresh = (res[...].astype(F32) + factor * (tot[...] * scale * gains[gain:gain + 1, :])).astype(BF16)
        res[...] = fresh
        for _, copy in copies:
            copy.wait_send()
        if last:
            return
        wide = fresh.astype(F32)
        scale = lax.rsqrt(jnp.sum(wide * wide, axis=-1, keepdims=True) / D + EPSILON)
        rows = pl.ds(pl.multiple_of(x * SHARE, SHARE), SHARE)
        copies = []
        for q in range(QN):
            cols = slice(q * QW, (q + 1) * QW)
            xn[q, rows, :] = (wide[:, cols] * scale * gains[gain + 1:gain + 2, cols]).astype(BF16)
            for d in (2, 1, 3):
                copy = pltpu.make_async_remote_copy(
                    src_ref=xn.at[q, rows, :], dst_ref=xn.at[q, rows, :],
                    send_sem=ag_send.at[layer, d - 1, q], recv_sem=ag_recv.at[layer, d - 1, q],
                    device_id=peers[d - 1], device_id_type=pl.DeviceIdType.MESH,
                )
                copy.start()
                copies.append(copy)
        for copy in copies:
            copy.wait()

    def ffn(layer, gain, last):
        for w in range(2):
            gate = project(wa, w, 0, HID)
            up = project(wb, w, 0, HID)
            hid[:, w * HID:(w + 1) * HID] = (gate / (1.0 + jnp.exp(-gate)) * up).astype(BF16)

        def parts(q):
            total = None
            for w in range(2):
                a = dot_t(hid[:, w * HID:w * HID + 128], weight(wa, w, q, HID, HID + 128))
                b = dot_t(hid[:, w * HID + 128:(w + 1) * HID], weight(wb, w, q, HID, HID + 256))
                total = a + b if total is None else total + a + b
            return total

        narrow(layer, parts, gain, 0.5, last)

    ffn(0, 1, False)

    gated, outer = [], []
    for w in range(2):
        low = project(wa, w, 512, 896)
        high = project(wb, w, 640, 896)
        both = jnp.concatenate([low, high], axis=1).astype(BF16).astype(F32)
        outer.append(both[:, 0:CH])
        product = both[:, CH:2 * CH] * both[:, 2 * CH:3 * CH]
        gated.append(product)
        halo_out[w, :, 0:CH] = product[HALF - 8:HALF, :]
    hcopy = pltpu.make_async_remote_copy(
        src_ref=halo_out, dst_ref=halo_in, send_sem=h_send, recv_sem=h_recv,
        device_id=mate, device_id_type=pl.DeviceIdType.MESH,
    )
    hcopy.start()
    hcopy.wait()
    row = lax.broadcasted_iota(jnp.int32, (HALF, CH), 0)
    for w in range(2):
        before = jnp.where(c == 1, halo_in[w, :, 0:CH], 0.0)
        one, two = before[7:8, :], before[6:7, :]
        g = gated[w]
        back1 = jnp.where(row == 0, one, pltpu.roll(g, 1, 0))
        back2 = pltpu.roll(g, 2, 0)
        back2 = jnp.where(row == 0, two, jnp.where(row == 1, one, back2))
        conv = taps[w, 0:1, 0:CH] * back2 + taps[w, 1:2, 0:CH] * back1 + taps[w, 2:3, 0:CH] * g
        mixed = outer[w] * conv
        hid[:, w * 256:(w + 1) * 256] = jnp.concatenate(
            [jnp.zeros((HALF, 12), F32), mixed, jnp.zeros((HALF, 112), F32)], axis=1
        ).astype(BF16)

    def mixer_parts(q):
        return dot_t(hid[:, 0:256], weight(wb, 0, q, 640, 896)) + dot_t(hid[:, 256:512], weight(wb, 1, q, 640, 896))

    narrow(1, mixer_parts, 3, 1.0, False)
    ffn(2, 5, True)

    acc[...] = jnp.zeros_like(acc)
    for j, base, width in windows():
        m = spread(j, base, width)
        acc[:, base:base + width] += dot_t(res[:, 384 * j:384 * (j + 1)], m)
    rows = pl.ds(pl.multiple_of(c * HALF + x * SHARE, SHARE), SHARE)
    fin[rows, :] = acc[:, 0:D].astype(BF16)
    outs = []

    def result(index, rows, dev, sems):
        return pltpu.make_async_remote_copy(
            src_ref=fin.at[rows, :], dst_ref=fin.at[rows, :], send_sem=sems[0].at[index], recv_sem=sems[1].at[index],
            device_id=dev, device_id_type=pl.DeviceIdType.MESH,
        )

    for d in (2, 1, 3):
        copy = result(d, rows, peers[d - 1], (fo_send, fo_recv))
        copy.start()
        outs.append(copy)
    copy = result(0, rows, mate, (fp_send, fp_recv))
    copy.start()
    mate_outs = [copy]
    for d in (1, 3, 2):
        theirs = pl.ds(pl.multiple_of(c * HALF + lax.rem(x + NX - d, NX) * SHARE, SHARE), SHARE)
        result(d, theirs, mate, (fo_send, fo_recv)).wait_recv()
        copy = result(d, theirs, mate, (fp_send, fp_recv))
        copy.start()
        mate_outs.append(copy)
    for copy in mate_outs:
        copy.wait_recv()
    back = pltpu.make_async_copy(fin, out, l_sem.at[0])
    back.start()
    for copy in started + mates + outs + mate_outs:
        copy.wait_send()
    back.wait()


def local(stream_in, norm_gains, gate_proj, up_proj, down_proj, outer_gate, inner_gate, value_proj, mixer_out, conv_taps):
    mix = jnp.concatenate([outer_gate, inner_gate, value_proj, mixer_out], axis=1)
    mix = jnp.pad(mix, ((0, 0), (0, 640 - 4 * CH)))
    rows = ((0, PAD - OWN), (0, 0))
    wa_in = jnp.pad(jnp.concatenate([gate_proj, down_proj[:, :128], mix[:, :384]], axis=1), rows)
    wb_in = jnp.pad(jnp.concatenate([up_proj, down_proj[:, 128:], mix[:, 384:]], axis=1), rows)
    gains = jnp.pad(norm_gains.reshape(6, 96, OWN), ((0, 2), (0, 0), (0, PAD - OWN))).reshape(8, DP)
    x = lax.axis_index("tp") // 2
    taps = lax.dynamic_slice_in_dim(conv_taps, x * 2 * CH, 2 * CH, 1).astype(F32)
    taps = jnp.pad(jnp.moveaxis(taps.reshape(3, 2, CH), 1, 0), ((0, 0), (0, 5), (0, 256 - CH)))
    vmem = pl.BlockSpec(memory_space=pltpu.VMEM)
    hbm = pl.BlockSpec(memory_space=pl.ANY)
    dma = pltpu.SemaphoreType.DMA
    return pl.pallas_call(
        kernel,
        out_shape=jax.ShapeDtypeStruct((2 * HALF, D), BF16),
        in_specs=[hbm, hbm, vmem, vmem, vmem],
        out_specs=hbm,
        scratch_shapes=[
            pltpu.VMEM((2, NZ, NY * PAD + 8, CW_A), BF16),
            pltpu.VMEM((2, NZ, NY * PAD + 8, CW_B), BF16),
            pltpu.VMEM((HALF, DP), BF16),
            pltpu.VMEM((QN, HALF, QW), BF16),
            pltpu.VMEM((HALF, 2 * HID), BF16),
            pltpu.VMEM((3, QN, HALF, QW), BF16),
            pltpu.VMEM((3, QN, SHARE, QW), BF16),
            pltpu.VMEM((SHARE, DP), F32),
            pltpu.VMEM((SHARE, DP), BF16),
            pltpu.VMEM((2 * HALF, D), BF16),
            pltpu.VMEM((SHARE, 2176), F32),
            pltpu.VMEM((2, 8, 256), F32),
            pltpu.VMEM((2, 8, 256), F32),
            dma((2, 96)), dma((2, 96)),
            dma((2, 12)), dma((2, 12)),
            dma((3, 3, 3)), dma((3, 3, 3)),
            dma((2, 3, 3)), dma((2, 3, 3)),
            dma((4,)), dma((4,)),
            dma((4,)), dma((4,)),
            dma(()), dma(()),
            dma((2,)),
        ],
        compiler_params=pltpu.CompilerParams(
            collective_id=0, has_side_effects=True, vmem_limit_bytes=58 * 1024 * 1024
        ),
        name="layer",
    )(wa_in, wb_in, stream_in, gains, taps)


def solution(mesh):
    return jax.shard_map(
        local,
        mesh=mesh,
        in_specs=(
            P("fs", None), P(), P("fs", "tp"), P("fs", "tp"), P("fs", "tp"),
            P("fs", "tp"), P("fs", "tp"), P("fs", "tp"), P("fs", "tp"), P(),
        ),
        out_specs=P("fs", None),
        check_vma=False,
    )
```

time: 342 us -> 150 us (0.44)
  waiting for transfers between devices: 166 us -> 0 us
  Pallas kernels: 0 us -> 138 us
  blocking collectives: 101 us -> 0 us
  matrix products: 21.8 us -> 0 us
  starting transfers between devices: 15.6 us -> 0 us
  between operations: 13.5 us -> 0.04 us
  local copies, waits for them, and re-layouts: 18.4 us -> 8.12 us
    pallas_call x0 -> x1, Pallas kernels: none -> 138 us  [local(): pl.pallas_call(kernel, out_shape=jax.ShapeDtypeStruct((2 * HALF, D), BF16...]
    all_gather x1 -> x0, waiting for transfers between devices: 138 us -> none  [in_one_piece(): lax.all_gather(both, axis, axis=dim, tiled=True)]
    all_to_all x5 -> x0, blocking collectives: 101 us -> none  [the longest x3 63.5 us: summed_on_arrival(): lax.all_to_all(in_blocks(shard, dim, devices), axis, 0, 0, tiled=True)]
    all_to_all x4 -> x0, waiting for transfers between devices: 28.2 us -> none  [copy_for_each(): lax.all_to_all(jnp.broadcast_to(shard[None], (devices, *shard.shape)), ax...]
    dot_general x7 -> x0, matrix products: 21.8 us -> none  [the longest x3 11 us: narrow(): lax.dot_general(inner, weight, (((1,), (1,)), ((), ())), preferred_elemen...]
    all_to_all x4 -> x0, starting transfers between devices: 15.6 us -> none  [copy_for_each(): lax.all_to_all(jnp.broadcast_to(shard[None], (devices, *shard.shape)), ax...]
    unnamed x4 -> x5, local copies, waits for them, and re-layouts: 12.4 us -> 2.2 us
  transfers between devices with their start and end apart: 5 -> 0, of which waited for: 5 -> 0; matrix products, arithmetic and copies ran while one was open for 1% -> 0% of each run, Pallas kernels for 0% -> 0%
where the time goes in v1:
time: 150 us
  Pallas kernels  138 us (92%)
  local copies, waits for them, and re-layouts  8.12 us (5%)
  other arithmetic  2.91 us (2%)
    pallas_call x1, Pallas kernels, local(): pl.pallas_call(kernel, out_shape=jax.ShapeDtypeStruct((2 * HALF, D), BF16...  138 us

profile of v1, /device:TPU:1, one launch (start us, length us, event | category | flops | bytes accessed | tf_op | source)
XLA Modules:
  0.0 149.5 jit_solution(6708856628403986082)
XLA Ops:
  0.0 0.0 copy-start
  0.0 0.0 copy-start.1
  0.0 0.7 copy-done
  0.7 0.1 constant_dynamic-slice_fusion
  0.8 0.1 reshape.12
  0.9 0.7 slice.14
  1.6 0.6 pad_convert_fusion.taps
  2.2 0.8 fusion.20
  3.0 0.7 slice.16
  3.7 1.5 %fusion.9 = (bf16[24,896]{1,0:T(8,128)(2,1)}, bf16[24,896]{1,0:T(8,128)(2,1)}) fusion(bf16[22,132]{1,0:T(8,128)(2,1)} %param.17, bf16[22,128]{1,0:T(8,128)(2,1)S(1)} %slice.14, bf16[22,384]{1,0:T(8,128)(2,1)} %param.12, bf16[22,132]{1,0:T(8,128)(2,1)} %param.16, bf16[22,132]{1,0:T(8,128)(2,1)} %param.15, bf16[22,256]{1,0:T(8,128)(2,1)S(1)} %fusion.20, ...), kind=kLoop, calls=%fused_computation.10 | loop fusion | flops 537600 | bytes 165392 | tf_op jit(solution)/shard_map/concatenate | solution.py:339
  5.2 1.2 reshape.10
  6.4 0.9 reshape.11.gains
  7.2 0.0 copy-done.1
  7.3 1.5 %copy.14.stream = bf16[256,2112]{1,0:T(8,128)(2,1)} copy(bf16[256,2112]{0,1:T(8,128)(2,1)S(1)} %copy-done.1) | data formatting | bytes 2162688 | tf_op args[0]
  8.7 138.4 %layer.1 = bf16[256,2112]{1,0:T(8,128)(2,1)} custom-call(bf16[24,896]{1,0:T(8,128)(2,1)} %get-tuple-element.5.wa_in, bf16[24,896]{1,0:T(8,128)(2,1)} %get-tuple-element.6.wb_in, bf16[256,2112]{1,0:T(8,128)(2,1)} %copy.14.stream, f32[8,2304]{1,0:T(8,128)} %reshape.11.gains, f32[2,8,256]{2,1,0:T(8,128)} %pad_convert_fusion.taps), custom_call_target="tpu_custom_call" | custom-call | tf_op jit(solution)/shard_map/layer/pallas_call | solution.py:348
  147.2 2.3 %copy.15 = bf16[256,2112]{0,1:T(8,128)(2,1)} copy(bf16[256,2112]{1,0:T(8,128)(2,1)} %layer.1) | data formatting | bytes 2162688 | tf_op jit(solution)/shard_map/layer/pallas_call | solution.py:348
  (2 shorter events, 0.0 us)
Async XLA Ops:
  0.0 0.7 copy-start
  0.0 7.2 %copy-start.1 = (bf16[256,2112]{0,1:T(8,128)(2,1)S(1)}, bf16[256,2112]{0,1:T(8,128)(2,1)}, u32[]{:S(2)}) copy-start(bf16[256,2112]{0,1:T(8,128)(2,1)} %param.10) | copy-start | bytes 3244036

commit v2 on v1

--- a/solution.py
+++ b/solution.py
@@ -14,7 +14,7 @@
 QN, QW = 3, DP // 3
 HALF, SHARE = 128, 32
 HID, CH = 384, 132
-CW_A, CW_B = 896, 896
+LAG = 5
 F32, BF16 = jnp.float32, jnp.bfloat16
 
 
@@ -45,8 +45,9 @@
 
 
 def kernel(
-    wa_in, wb_in, stream, gains, taps, out,
-    wa, wb, xs, xn, hid, part, got, tot, res, fin, acc, halo_out, halo_in,
+    gate_in, up_in, down_in, outer_in, inner_in, value_in, mixer_in, stream_in, gains_in, taps_in, out,
+    gate_sh, up_sh, down_sh, outer_sh, inner_sh, value_sh, mixer_sh, stream, gains_raw, taps_raw,
+    wa, wb, ma, mb, xs, xn, proj, hid, part, got, tot, res, fin, acc, fout, gains, taps, halo_out, halo_in,
     g_send, g_recv, p_send, p_recv, rs_send, rs_recv, ag_send, ag_recv,
     fo_send, fo_recv, fp_send, fp_recv, h_send, h_recv, l_sem,
 ):
@@ -64,9 +65,14 @@
     def zmod(v):
         return lax.rem(v + NZ, NZ)
 
-    here = [wa.at[c, z, pl.ds(pl.multiple_of(y * PAD, 8), PAD), :], wb.at[c, z, pl.ds(pl.multiple_of(y * PAD, 8), PAD), :]]
-    own = [pltpu.make_async_copy(src, dst, l_sem.at[i]) for i, (src, dst) in enumerate(zip((wa_in, wb_in), here))]
-    for copy in own:
+    arrivals = [
+        pltpu.make_async_copy(src, dst, l_sem.at[i])
+        for i, (src, dst) in enumerate((
+            (gate_in, gate_sh), (up_in, up_sh), (down_in, down_sh), (outer_in, outer_sh), (inner_in, inner_sh),
+            (value_in, value_sh), (mixer_in, mixer_sh), (stream_in, stream), (gains_in, gains_raw), (taps_in, taps_raw),
+        ))
+    ]
+    for copy in arrivals:
         copy.start()
 
     y_fwd, y_back = at(z, ymod(y + s), x, c), at(z, ymod(y - s), x, c)
@@ -76,13 +82,28 @@
     barrier = pltpu.get_barrier_semaphore()
     for dev in [y_fwd, y_back, z_fwd, z_back, mate] + peers:
         pl.semaphore_signal(barrier, inc=1, device_id=dev, device_id_type=pl.DeviceIdType.MESH)
+    for copy in arrivals[:7]:
+        copy.wait()
+
+    def rows24(ref):
+        return jnp.concatenate([ref[...].astype(F32), jnp.zeros((PAD - OWN, ref.shape[1]), F32)], axis=0)
+
+    here = pl.ds(pl.multiple_of(y * PAD, 8), PAD)
+    wa[c, z, here, 0:HID] = rows24(gate_sh).astype(BF16)
+    wb[c, z, here, 0:HID] = rows24(up_sh).astype(BF16)
+    down = rows24(down_sh).astype(BF16)
+    wa[c, z, here, HID:HID + 128] = down[:, 0:128]
+    wb[c, z, here, HID:HID + 256] = down[:, 128:HID]
+    mix = jnp.concatenate(
+        [rows24(outer_sh), rows24(inner_sh), rows24(value_sh), rows24(mixer_sh), jnp.zeros((PAD, 640 - 4 * CH), F32)], axis=1
+    ).astype(BF16)
+    ma[c, z, here, :] = mix[:, 0:384]
+    mb[c, z, here, :] = mix[:, 384:640]
     pl.semaphore_wait(barrier, 8)
-    for copy in own:
-        copy.wait()
 
     ys = [y] + [ymod(y - s * d) for d in range(1, 5)] + [ymod(y + s * d) for d in range(1, 4)]
     zs = [z] + [zmod(z - s * d) for d in range(1, 7)] + [zmod(z + s * d) for d in range(1, 6)]
-    bufs = (wa, wb)
+    bufs = (wa, wb, ma, mb)
 
     def remote(which, src_zz, src_yy, index, dev):
         ref = bufs[which].at[c, src_zz, pl.ds(pl.multiple_of(src_yy * PAD, 8), PAD), :]
@@ -127,73 +148,120 @@
     mates = []
 
     def to_mate(which, sub, index):
-        ref = bufs[which].at[c, zs[index], pl.ds(0, NY * PAD), :] if which == 0 else sub
+        ref = bufs[which].at[c, zs[index], pl.ds(0, NY * PAD), :] if which % 2 == 0 else sub
         copy = pltpu.make_async_remote_copy(
             src_ref=ref, dst_ref=ref, send_sem=p_send.at[which, index], recv_sem=p_recv.at[which, index],
             device_id=mate, device_id_type=pl.DeviceIdType.MESH,
         )
         copy.start()
-        mates.append(copy)
+        mates.append((which, copy))
 
     y_order = [0, 1, 5, 2, 6, 3, 7, 4]
     z_order = [0, 1, 7, 2, 8, 3, 9, 4, 10, 5, 11, 6]
 
-    z_next(0, 0, 0)
-    y_next(1, 0, 0)
-    y_next(0, 0, 0)
-    z_next(1, 0, 0)
-
-    half = stream[pl.ds(pl.multiple_of(c * HALF, HALF), HALF), :]
-    mine = stream[pl.ds(pl.multiple_of(c * HALF + x * SHARE, SHARE), SHARE), :]
-    for j, base, width in windows():
-        m = spread(j, base, width)
-        xs[:, 384 * j:384 * (j + 1)] = dot(half[:, base:base + width], m).astype(BF16)
-        res[:, 384 * j:384 * (j + 1)] = dot(mine[:, base:base + width], m).astype(BF16)
-    wide = xs[...].astype(F32)
-    scale = lax.rsqrt(jnp.sum(wide * wide, axis=-1, keepdims=True) / D + EPSILON)
-    for q in range(QN):
-        cols = slice(q * QW, (q + 1) * QW)
-        xn[q] = (wide[:, cols] * scale * gains[0:1, cols]).astype(BF16)
-
-    for slot in range(1, 11):
+    def own_out(group):
+        even, odd = 2 * group, 2 * group + 1
+        z_next(even, 0, 0)
+        y_next(odd, 0, 0)
+        y_next(even, 0, 0)
+        z_next(odd, 0, 0)
+
+    def slot_of(group, slot):
+        even, odd = 2 * group, 2 * group + 1
         for jy in y_order:
             if y_far(jy) == slot:
-                take(0, 0, jy)
-                z_next(0, 0, jy)
-                y_next(0, 0, jy)
+                take(even, 0, jy)
+                z_next(even, 0, jy)
+                y_next(even, 0, jy)
         for jz in z_order:
             if z_far(jz) == slot:
-                take(1, jz, 0)
-                y_next(1, jz, 0)
-                z_next(1, jz, 0)
+                take(odd, jz, 0)
+                y_next(odd, jz, 0)
+                z_next(odd, jz, 0)
         for jz in z_order:
             for jy in y_order:
                 if y_far(jy) + z_far(jz) == slot:
                     if jz > 0:
-                        take(0, jz, jy)
-                        z_next(0, jz, jy)
+                        take(even, jz, jy)
+                        z_next(even, jz, jy)
                     if jy > 0:
-                        take(1, jz, jy)
-                        y_next(1, jz, jy)
+                        take(odd, jz, jy)
+                        y_next(odd, jz, jy)
         for jz in range(NZ):
             if slot == 4 + z_far(jz):
-                to_mate(0, None, jz)
+                to_mate(even, None, jz)
         for jy in range(NY):
             if slot == 6 + y_far(jy):
-                to_mate(1, wb.at[c, :, pl.ds(pl.multiple_of(ys[jy] * PAD, 8), PAD), :], jy)
-    for copy in mates:
-        copy.wait_recv()
+                to_mate(odd, bufs[odd].at[c, :, pl.ds(pl.multiple_of(ys[jy] * PAD, 8), PAD), :], jy)
+
+    def complete(group):
+        for which, copy in mates:
+            if which // 2 == group:
+                copy.wait_recv()
+
+    def window(j, base, width):
+        m = spread(j, base, width)
+        to = slice(384 * j, 384 * (j + 1))
+        half = stream[base:base + width, pl.ds(pl.multiple_of(c * HALF, HALF), HALF)]
+        xs[:, to] = lax.dot_general(half, m, (((0,), (0,)), ((), ())), preferred_element_type=F32).astype(BF16)
+        res[:, to] = xs[pl.ds(pl.multiple_of(x * SHARE, SHARE), SHARE), to]
+        left = gains_raw[:, base:base + width]
+        total = None
+        for _ in range(3):
+            term = left.astype(BF16)
+            left = left - term.astype(F32)
+            moved = dot(term, m)
+            total = moved if total is None else total + moved
+        gains[0:6, to] = total
+
+    def first_norm():
+        wide = xs[...].astype(F32)
+        scale = lax.rsqrt(jnp.sum(wide * wide, axis=-1, keepdims=True) / D + EPSILON)
+        for q in range(QN):
+            cols = slice(q * QW, (q + 1) * QW)
+            xn[q] = (wide[:, cols] * scale * gains[0:1, cols]).astype(BF16)
+
+    def own_taps():
+        for w in range(2):
+            row = lax.broadcasted_iota(jnp.int32, (8 * CH, 256), 0)
+            col = lax.broadcasted_iota(jnp.int32, (8 * CH, 256), 1)
+            pick = jnp.where((row == col + (2 * x + w) * CH) & (col < CH), 1.0, 0.0).astype(BF16)
+            taps[w, 0:3, :] = dot(taps_raw[...], pick)
+
+    own_out(0)
+    for copy in arrivals[7:]:
+        copy.wait()
+    for slot in range(1, 11):
+        slot_of(0, slot)
+        if slot > LAG:
+            slot_of(1, slot - LAG)
+        if slot == LAG:
+            own_out(1)
+        if slot <= 6:
+            window(*windows()[slot - 1])
+        if slot == 7:
+            first_norm()
+        if slot == 8:
+            own_taps()
+    later = list(range(11 - LAG, 11))
+    complete(0)
 
     def weight(buf, w, q, lo, hi):
         return buf[w, 4 * q:4 * q + 4, 0:NY * PAD, lo:hi].reshape(QW, hi - lo)
 
-    def project(buf, w, lo, hi):
-        total = dot(xn[0], weight(buf, w, 0, lo, hi))
-        for q in range(1, QN):
-            total = total + dot(xn[q], weight(buf, w, q, lo, hi))
-        return total
-
-    def narrow(layer, parts, gain, factor, last):
+    def project(terms, incoming):
+        for q in range(QN):
+            for at_q, copy in incoming:
+                if at_q == q:
+                    copy.wait()
+            for i, (buf, w, lo, hi) in enumerate(terms):
+                value = dot(xn[q], weight(buf, w, q, lo, hi))
+                if q == 0:
+                    proj[i, :, 0:hi - lo] = value
+                else:
+                    proj[i, :, 0:hi - lo] += value
+
+    def narrow(layer, parts, gain, factor, last, between=(), after=()):
         copies = []
         for q in range(QN):
             total = parts(q)
@@ -208,6 +276,8 @@
                 )
                 copy.start()
                 copies.append((q, copy))
+        for slot in between:
+            slot_of(1, slot)
         squares = jnp.zeros((SHARE, 1), F32)
         for q in range(QN):
             for at_q, copy in copies:
@@ -224,7 +294,7 @@
         for _, copy in copies:
             copy.wait_send()
         if last:
-            return
+            return []
         wide = fresh.astype(F32)
         scale = lax.rsqrt(jnp.sum(wide * wide, axis=-1, keepdims=True) / D + EPSILON)
         rows = pl.ds(pl.multiple_of(x * SHARE, SHARE), SHARE)
@@ -239,14 +309,17 @@
                     device_id=peers[d - 1], device_id_type=pl.DeviceIdType.MESH,
                 )
                 copy.start()
-                copies.append(copy)
-        for copy in copies:
-            copy.wait()
-
-    def ffn(layer, gain, last):
+                copies.append((q, copy))
+        for slot in after:
+            slot_of(1, slot)
+        return copies
+
+    def ffn(layer, gain, last, incoming, first=(), between=(), after=()):
+        project(((wa, 0, 0, HID), (wb, 0, 0, HID), (wa, 1, 0, HID), (wb, 1, 0, HID)), incoming)
+        for slot in first:
+            slot_of(1, slot)
         for w in range(2):
-            gate = project(wa, w, 0, HID)
-            up = project(wb, w, 0, HID)
+            gate, up = proj[2 * w], proj[2 * w + 1]
             hid[:, w * HID:(w + 1) * HID] = (gate / (1.0 + jnp.exp(-gate)) * up).astype(BF16)
 
         def parts(q):
@@ -257,15 +330,15 @@
                 total = a + b if total is None else total + a + b
             return total
 
-        narrow(layer, parts, gain, 0.5, last)
-
-    ffn(0, 1, False)
+        return narrow(layer, parts, gain, 0.5, last, between, after)
+
+    incoming = ffn(0, 1, False, [], later[:1], later[1:3], later[3:])
+    complete(1)
 
     gated, outer = [], []
+    project(((ma, 0, 0, 384), (mb, 0, 0, 256), (ma, 1, 0, 384), (mb, 1, 0, 256)), incoming)
     for w in range(2):
-        low = project(wa, w, 512, 896)
-        high = project(wb, w, 640, 896)
-        both = jnp.concatenate([low, high], axis=1).astype(BF16).astype(F32)
+        both = jnp.concatenate([proj[2 * w], proj[2 * w + 1, :, 0:256]], axis=1).astype(BF16).astype(F32)
         outer.append(both[:, 0:CH])
         product = both[:, CH:2 * CH] * both[:, 2 * CH:3 * CH]
         gated.append(product)
@@ -291,18 +364,13 @@
         ).astype(BF16)
 
     def mixer_parts(q):
-        return dot_t(hid[:, 0:256], weight(wb, 0, q, 640, 896)) + dot_t(hid[:, 256:512], weight(wb, 1, q, 640, 896))
-
-    narrow(1, mixer_parts, 3, 1.0, False)
-    ffn(2, 5, True)
-
-    acc[...] = jnp.zeros_like(acc)
-    for j, base, width in windows():
-        m = spread(j, base, width)
-        acc[:, base:base + width] += dot_t(res[:, 384 * j:384 * (j + 1)], m)
-    rows = pl.ds(pl.multiple_of(c * HALF + x * SHARE, SHARE), SHARE)
-    fin[rows, :] = acc[:, 0:D].astype(BF16)
-    outs = []
+        return dot_t(hid[:, 0:256], weight(mb, 0, q, 0, 256)) + dot_t(hid[:, 256:512], weight(mb, 1, q, 0, 256))
+
+    incoming = narrow(1, mixer_parts, 3, 1.0, False)
+    ffn(2, 5, True, incoming)
+
+    def mine_of(half, d):
+        return pl.ds(pl.multiple_of(half * HALF + lax.rem(x + NX - d, NX) * SHARE, SHARE), SHARE)
 
     def result(index, rows, dev, sems):
         return pltpu.make_async_remote_copy(
@@ -310,74 +378,79 @@
             device_id=dev, device_id_type=pl.DeviceIdType.MESH,
         )
 
+    fin[mine_of(c, 0), :] = res[...]
+    outs, mate_outs = [], []
     for d in (2, 1, 3):
-        copy = result(d, rows, peers[d - 1], (fo_send, fo_recv))
-        copy.start()
-        outs.append(copy)
-    copy = result(0, rows, mate, (fp_send, fp_recv))
-    copy.start()
-    mate_outs = [copy]
-    for d in (1, 3, 2):
-        theirs = pl.ds(pl.multiple_of(c * HALF + lax.rem(x + NX - d, NX) * SHARE, SHARE), SHARE)
-        result(d, theirs, mate, (fo_send, fo_recv)).wait_recv()
-        copy = result(d, theirs, mate, (fp_send, fp_recv))
-        copy.start()
-        mate_outs.append(copy)
-    for copy in mate_outs:
-        copy.wait_recv()
-    back = pltpu.make_async_copy(fin, out, l_sem.at[0])
-    back.start()
-    for copy in started + mates + outs + mate_outs:
+        outs.append(result(d, mine_of(c, 0), peers[d - 1], (fo_send, fo_recv)))
+        outs[-1].start()
+    for d in (0, 1, 3, 2):
+        if d > 0:
+            result(d, mine_of(c, d), mate, (fo_send, fo_recv)).wait_recv()
+        mate_outs.append(result(d, mine_of(c, d), mate, (fp_send, fp_recv)))
+        mate_outs[-1].start()
+    backs = []
+    for turn, h in enumerate((c, 1 - c)):
+        if turn == 1:
+            for copy in mate_outs:
+                copy.wait_recv()
+        tokens = pl.ds(pl.multiple_of(h * HALF, HALF), HALF)
+        acc[...] = jnp.zeros_like(acc)
+        for j, base, width in windows():
+            acc[base:base + width, :] += dot_t(spread(j, base, width), fin[tokens, 384 * j:384 * (j + 1)])
+        fout[turn] = acc[...].astype(BF16)
+        backs.append(pltpu.make_async_copy(fout.at[turn], out.at[:, tokens], l_sem.at[turn]))
+        backs[-1].start()
+    for copy in started + [copy for _, copy in mates] + outs + mate_outs:
         copy.wait_send()
-    back.wait()
+    for copy in backs:
+        copy.wait()
 
 
 def local(stream_in, norm_gains, gate_proj, up_proj, down_proj, outer_gate, inner_gate, value_proj, mixer_out, conv_taps):
-    mix = jnp.concatenate([outer_gate, inner_gate, value_proj, mixer_out], axis=1)
-    mix = jnp.pad(mix, ((0, 0), (0, 640 - 4 * CH)))
-    rows = ((0, PAD - OWN), (0, 0))
-    wa_in = jnp.pad(jnp.concatenate([gate_proj, down_proj[:, :128], mix[:, :384]], axis=1), rows)
-    wb_in = jnp.pad(jnp.concatenate([up_proj, down_proj[:, 128:], mix[:, 384:]], axis=1), rows)
-    gains = jnp.pad(norm_gains.reshape(6, 96, OWN), ((0, 2), (0, 0), (0, PAD - OWN))).reshape(8, DP)
-    x = lax.axis_index("tp") // 2
-    taps = lax.dynamic_slice_in_dim(conv_taps, x * 2 * CH, 2 * CH, 1).astype(F32)
-    taps = jnp.pad(jnp.moveaxis(taps.reshape(3, 2, CH), 1, 0), ((0, 0), (0, 5), (0, 256 - CH)))
-    vmem = pl.BlockSpec(memory_space=pltpu.VMEM)
     hbm = pl.BlockSpec(memory_space=pl.ANY)
     dma = pltpu.SemaphoreType.DMA
     return pl.pallas_call(
         kernel,
-        out_shape=jax.ShapeDtypeStruct((2 * HALF, D), BF16),
-        in_specs=[hbm, hbm, vmem, vmem, vmem],
+        out_shape=jax.ShapeDtypeStruct((D, 2 * HALF), BF16),
+        in_specs=[hbm] * 10,
         out_specs=hbm,
         scratch_shapes=[
-            pltpu.VMEM((2, NZ, NY * PAD + 8, CW_A), BF16),
-            pltpu.VMEM((2, NZ, NY * PAD + 8, CW_B), BF16),
+            pltpu.VMEM((OWN, HID), BF16), pltpu.VMEM((OWN, HID), BF16), pltpu.VMEM((OWN, HID), BF16),
+            pltpu.VMEM((OWN, CH), BF16), pltpu.VMEM((OWN, CH), BF16), pltpu.VMEM((OWN, CH), BF16), pltpu.VMEM((OWN, CH), BF16),
+            pltpu.VMEM((D, 2 * HALF), BF16), pltpu.VMEM((6, D), F32), pltpu.VMEM((3, 8 * CH), BF16),
+            pltpu.VMEM((2, NZ, NY * PAD + 8, 512), BF16),
+            pltpu.VMEM((2, NZ, NY * PAD + 8, 640), BF16),
+            pltpu.VMEM((2, NZ, NY * PAD + 8, 384), BF16),
+            pltpu.VMEM((2, NZ, NY * PAD + 8, 256), BF16),
             pltpu.VMEM((HALF, DP), BF16),
             pltpu.VMEM((QN, HALF, QW), BF16),
+            pltpu.VMEM((4, HALF, HID), F32),
             pltpu.VMEM((HALF, 2 * HID), BF16),
             pltpu.VMEM((3, QN, HALF, QW), BF16),
             pltpu.VMEM((3, QN, SHARE, QW), BF16),
             pltpu.VMEM((SHARE, DP), F32),
             pltpu.VMEM((SHARE, DP), BF16),
-            pltpu.VMEM((2 * HALF, D), BF16),
-            pltpu.VMEM((SHARE, 2176), F32),
+            pltpu.VMEM((2 * HALF, DP), BF16),
+            pltpu.VMEM((D, HALF), F32),
+            pltpu.VMEM((2, D, HALF), BF16),
+            pltpu.VMEM((8, DP), F32),
             pltpu.VMEM((2, 8, 256), F32),
             pltpu.VMEM((2, 8, 256), F32),
-            dma((2, 96)), dma((2, 96)),
-            dma((2, 12)), dma((2, 12)),
+            pltpu.VMEM((2, 8, 256), F32),
+            dma((4, 96)), dma((4, 96)),
+            dma((4, 12)), dma((4, 12)),
             dma((3, 3, 3)), dma((3, 3, 3)),
             dma((2, 3, 3)), dma((2, 3, 3)),
             dma((4,)), dma((4,)),
             dma((4,)), dma((4,)),
             dma(()), dma(()),
-            dma((2,)),
+            dma((10,)),
         ],
         compiler_params=pltpu.CompilerParams(
             collective_id=0, has_side_effects=True, vmem_limit_bytes=58 * 1024 * 1024
         ),
         name="layer",
-    )(wa_in, wb_in, stream_in, gains, taps)
+    )(gate_proj, up_proj, down_proj, outer_gate, inner_gate, value_proj, mixer_out, stream_in.T, norm_gains, conv_taps).T
 
 
 def solution(mesh):

time: 150 us -> 134 us (0.89)
  Pallas kernels: 138 us -> 132 us
  local copies, waits for them, and re-layouts: 8.12 us -> 2.29 us
  other arithmetic: 2.91 us -> 0 us
    pallas_call x1, Pallas kernels: 138 us -> 132 us  [local(): pl.pallas_call(kernel, out_shape=jax.ShapeDtypeStruct((D, 2 * HALF), BF16...]
    pallas_call x1 -> x0, local copies, waits for them, and re-layouts: 2.31 us -> none  [local(): pl.pallas_call(kernel, out_shape=jax.ShapeDtypeStruct((2 * HALF, D), BF16...]
    concatenate x2 -> x0, other arithmetic: 2.31 us -> none  [the longest x1 1.5 us: local(): jnp.concatenate([gate_proj, down_proj[:, :128], mix[:, :384]], axis=1)]
    reshape x4 -> x0, local copies, waits for them, and re-layouts: 2.1 us -> none  [the longest x1 1.15 us: local(): norm_gains.reshape(6, 96, OWN)]
where the time goes in v2:
time: 134 us
  Pallas kernels  132 us (99%)
  local copies, waits for them, and re-layouts  2.29 us (2%)
    pallas_call x1, Pallas kernels, local(): pl.pallas_call(kernel, out_shape=jax.ShapeDtypeStruct((D, 2 * HALF), BF16...  132 us

profile of v2, /device:TPU:1, one launch (start us, length us, event | category | flops | bytes accessed | tf_op | source)
XLA Modules:
  0.0 134.2 jit_solution(12310246327994043445)
XLA Ops:
  0.0 131.9 %layer.1 = bf16[2112,256]{1,0:T(8,128)(2,1)} custom-call(bf16[22,384]{1,0:T(8,128)(2,1)} %gate_in.1, bf16[22,384]{1,0:T(8,128)(2,1)} %up_in.1, bf16[22,384]{1,0:T(8,128)(2,1)} %down_in.1, bf16[22,132]{1,0:T(8,128)(2,1)} %outer_in.1, bf16[22,132]{1,0:T(8,128)(2,1)} %inner_in.1, bf16[22,132]{1,0:T(8,128)(2,1)} %value_in.1, bf16[22,132]{1,0:T(8,128)(2,1)} %mixer_in.1, ...), custom_call_target="tpu_custom_call" | custom-call | tf_op jit(solution)/shard_map/layer/pallas_call | solution.py:412
  131.9 2.3 %copy.12 = bf16[256,2112]{0,1:T(8,128)(2,1)} copy(bf16[256,2112]{0,1:T(8,128)(2,1)} %bitcast.2) | data formatting | bytes 2162688

commit v3 on v2

--- a/solution.py
+++ b/solution.py
@@ -12,7 +12,8 @@
 PAD = 24
 DP = 96 * PAD
 QN, QW = 3, DP // 3
-HALF, SHARE = 128, 32
+GROUPS, HALF = 2, 128
+ROWS, SHARE = HALF // GROUPS, 16
 HID, CH = 384, 132
 LAG = 5
 F32, BF16 = jnp.float32, jnp.bfloat16
@@ -168,25 +169,20 @@
 
     def slot_of(group, slot):
         even, odd = 2 * group, 2 * group + 1
-        for jy in y_order:
-            if y_far(jy) == slot:
-                take(even, 0, jy)
-                z_next(even, 0, jy)
-                y_next(even, 0, jy)
-        for jz in z_order:
-            if z_far(jz) == slot:
-                take(odd, jz, 0)
-                y_next(odd, jz, 0)
-                z_next(odd, jz, 0)
-        for jz in z_order:
-            for jy in y_order:
-                if y_far(jy) + z_far(jz) == slot:
-                    if jz > 0:
-                        take(even, jz, jy)
-                        z_next(even, jz, jy)
-                    if jy > 0:
-                        take(odd, jz, jy)
-                        y_next(odd, jz, jy)
+        first = [(0, jy) for jy in y_order[1:]] + [(jz, jy) for jz in z_order[1:] for jy in y_order]
+        second = [(jz, 0) for jz in z_order[1:]] + [(jz, jy) for jy in y_order[1:] for jz in z_order]
+        first, second = (
+            [(jz, jy) for jz, jy in blocks if z_far(jz) + y_far(jy) == slot] for blocks in (first, second)
+        )
+        for i in range(max(len(first), len(second))):
+            for which, blocks in ((even, first), (odd, second)):
+                if i < len(blocks):
+                    jz, jy = blocks[i]
+                    take(which, jz, jy)
+                    if which == even or jy == 0:
+                        z_next(which, jz, jy)
+                    if which == odd or jz == 0:
+                        y_next(which, jz, jy)
         for jz in range(NZ):
             if slot == 4 + z_far(jz):
                 to_mate(even, None, jz)
@@ -199,12 +195,19 @@
             if which // 2 == group:
                 copy.wait_recv()
 
+    def token_rows(g, core, part_of, size):
+        return pl.ds(pl.multiple_of((2 * g + core) * ROWS + part_of * SHARE, SHARE), size)
+
     def window(j, base, width):
         m = spread(j, base, width)
         to = slice(384 * j, 384 * (j + 1))
-        half = stream[base:base + width, pl.ds(pl.multiple_of(c * HALF, HALF), HALF)]
-        xs[:, to] = lax.dot_general(half, m, (((0,), (0,)), ((), ())), preferred_element_type=F32).astype(BF16)
-        res[:, to] = xs[pl.ds(pl.multiple_of(x * SHARE, SHARE), SHARE), to]
+        everyone = lax.dot_general(
+            stream[base:base + width, :], m, (((0,), (0,)), ((), ())), preferred_element_type=F32
+        )
+        fin[:, to] = everyone.astype(BF16)
+        for g in range(GROUPS):
+            xs[g * ROWS:(g + 1) * ROWS, to] = fin[token_rows(g, c, 0, ROWS), to]
+            res[g, :, to] = fin[token_rows(g, c, x, SHARE), to]
         left = gains_raw[:, base:base + width]
         total = None
         for _ in range(3):
@@ -246,160 +249,177 @@
     later = list(range(11 - LAG, 11))
     complete(0)
 
-    def weight(buf, w, q, lo, hi):
-        return buf[w, 4 * q:4 * q + 4, 0:NY * PAD, lo:hi].reshape(QW, hi - lo)
-
-    def project(terms, incoming):
+    def weights(q, pieces):
+        return jnp.concatenate(
+            [buf[w, 4 * q:4 * q + 4, 0:NY * PAD, lo:hi].reshape(QW, hi - lo) for buf, w, lo, hi in pieces], axis=1
+        )
+
+    def mine(g, who):
+        return pl.ds(pl.multiple_of(g * ROWS + who * SHARE, SHARE), SHARE)
+
+    incoming, reduced = {}, {}
+
+    def project(layer, g, terms):
+        rows = slice(g * ROWS, (g + 1) * ROWS)
         for q in range(QN):
-            for at_q, copy in incoming:
-                if at_q == q:
-                    copy.wait()
-            for i, (buf, w, lo, hi) in enumerate(terms):
-                value = dot(xn[q], weight(buf, w, q, lo, hi))
+            for copy in incoming.get((layer, g, q), ()):
+                copy.wait()
+            for i, (buf, hi) in enumerate(terms):
+                value = dot(xn[q, rows, :], weights(q, [(buf, w, 0, hi) for w in range(2)]))
                 if q == 0:
-                    proj[i, :, 0:hi - lo] = value
+                    proj[g, i, :, 0:2 * hi] = value
                 else:
-                    proj[i, :, 0:hi - lo] += value
-
-    def narrow(layer, parts, gain, factor, last, between=(), after=()):
-        copies = []
+                    proj[g, i, :, 0:2 * hi] += value
+
+    def scatter(layer, g, parts):
         for q in range(QN):
-            total = parts(q)
-            part[layer, q] = total.astype(BF16)
+            part[layer, q, g * ROWS:(g + 1) * ROWS, :] = parts(q).astype(BF16)
             for d in (2, 1, 3):
-                there = lax.rem(x + d, NX)
                 copy = pltpu.make_async_remote_copy(
-                    src_ref=part.at[layer, q, pl.ds(pl.multiple_of(there * SHARE, SHARE), SHARE), :],
-                    dst_ref=got.at[d - 1, q],
-                    send_sem=rs_send.at[layer, d - 1, q], recv_sem=rs_recv.at[layer, d - 1, q],
+                    src_ref=part.at[layer, q, mine(g, lax.rem(x + d, NX)), :],
+                    dst_ref=got.at[g, d - 1, q],
+                    send_sem=rs_send.at[layer, g, d - 1, q], recv_sem=rs_recv.at[layer, g, d - 1, q],
                     device_id=peers[d - 1], device_id_type=pl.DeviceIdType.MESH,
                 )
                 copy.start()
-                copies.append((q, copy))
-        for slot in between:
-            slot_of(1, slot)
+                reduced.setdefault((layer, g, q), []).append(copy)
+
+    def settle(layer, g, gain, factor):
         squares = jnp.zeros((SHARE, 1), F32)
         for q in range(QN):
-            for at_q, copy in copies:
-                if at_q == q:
-                    copy.wait_recv()
-            total = part[layer, q, pl.ds(pl.multiple_of(x * SHARE, SHARE), SHARE), :].astype(F32)
+            for copy in reduced[layer, g, q]:
+                copy.wait_recv()
+            total = part[layer, q, mine(g, x), :].astype(F32)
             for d in range(3):
-                total = total + got[d, q].astype(F32)
+                total = total + got[g, d, q].astype(F32)
             tot[:, q * QW:(q + 1) * QW] = total
             squares = squares + jnp.sum(total * total, axis=-1, keepdims=True)
         scale = lax.rsqrt(squares / D + EPSILON)
-        fresh = (res[...].astype(F32) + factor * (tot[...] * scale * gains[gain:gain + 1, :])).astype(BF16)
-        res[...] = fresh
-        for _, copy in copies:
-            copy.wait_send()
-        if last:
-            return []
+        fresh = (res[g].astype(F32) + factor * (tot[...] * scale * gains[gain:gain + 1, :])).astype(BF16)
+        res[g] = fresh
+        return fresh
+
+    def spread_rows(layer, g, gain, fresh):
         wide = fresh.astype(F32)
         scale = lax.rsqrt(jnp.sum(wide * wide, axis=-1, keepdims=True) / D + EPSILON)
-        rows = pl.ds(pl.multiple_of(x * SHARE, SHARE), SHARE)
-        copies = []
+        rows = mine(g, x)
         for q in range(QN):
             cols = slice(q * QW, (q + 1) * QW)
-            xn[q, rows, :] = (wide[:, cols] * scale * gains[gain + 1:gain + 2, cols]).astype(BF16)
+            xn[q, rows, :] = (wide[:, cols] * scale * gains[gain:gain + 1, cols]).astype(BF16)
             for d in (2, 1, 3):
                 copy = pltpu.make_async_remote_copy(
                     src_ref=xn.at[q, rows, :], dst_ref=xn.at[q, rows, :],
-                    send_sem=ag_send.at[layer, d - 1, q], recv_sem=ag_recv.at[layer, d - 1, q],
+                    send_sem=ag_send.at[layer, g, d - 1, q], recv_sem=ag_recv.at[layer, g, d - 1, q],
                     device_id=peers[d - 1], device_id_type=pl.DeviceIdType.MESH,
                 )
                 copy.start()
-                copies.append((q, copy))
-        for slot in after:
-            slot_of(1, slot)
-        return copies
-
-    def ffn(layer, gain, last, incoming, first=(), between=(), after=()):
-        project(((wa, 0, 0, HID), (wb, 0, 0, HID), (wa, 1, 0, HID), (wb, 1, 0, HID)), incoming)
-        for slot in first:
-            slot_of(1, slot)
+                incoming.setdefault((layer + 1, g, q), []).append(copy)
+
+    def ffn(layer, g):
+        project(layer, g, ((wa, HID), (wb, HID)))
+        rows = slice(g * ROWS, (g + 1) * ROWS)
+        gate, up = proj[g, 0], proj[g, 1]
+        hid[rows, :] = (gate / (1.0 + jnp.exp(-gate)) * up).astype(BF16)
+
+        def parts(q):
+            down = [piece for w in range(2) for piece in ((wa, w, HID, HID + 128), (wb, w, HID, HID + 256))]
+            return dot_t(hid[rows, :], weights(q, down))
+
+        scatter(layer, g, parts)
+
+    halos = []
+
+    def mixer(g):
+        project(1, g, ((ma, 384), (mb, 128)))
+        gated, outer = [], []
         for w in range(2):
-            gate, up = proj[2 * w], proj[2 * w + 1]
-            hid[:, w * HID:(w + 1) * HID] = (gate / (1.0 + jnp.exp(-gate)) * up).astype(BF16)
-
-        def parts(q):
-            total = None
-            for w in range(2):
-                a = dot_t(hid[:, w * HID:w * HID + 128], weight(wa, w, q, HID, HID + 128))
-                b = dot_t(hid[:, w * HID + 128:(w + 1) * HID], weight(wb, w, q, HID, HID + 256))
-                total = a + b if total is None else total + a + b
-            return total
-
-        return narrow(layer, parts, gain, 0.5, last, between, after)
-
-    incoming = ffn(0, 1, False, [], later[:1], later[1:3], later[3:])
+            both = jnp.concatenate(
+                [proj[g, 0, :, w * 384:(w + 1) * 384], proj[g, 1, :, w * 128:(w + 1) * 128]], axis=1
+            ).astype(BF16).astype(F32)
+            outer.append(both[:, 0:CH])
+            product = both[:, CH:2 * CH] * both[:, 2 * CH:3 * CH]
+            gated.append(product)
+            halo_out[g, w, :, 0:CH] = product[ROWS - 8:ROWS, :]
+        copy = pltpu.make_async_remote_copy(
+            src_ref=halo_out.at[g], dst_ref=halo_in.at[g], send_sem=h_send.at[g], recv_sem=h_recv.at[g],
+            device_id=mate, device_id_type=pl.DeviceIdType.MESH,
+        )
+        copy.start()
+        copy.wait()
+        row = lax.broadcasted_iota(jnp.int32, (ROWS, CH), 0)
+        for w in range(2):
+            other = jnp.zeros((8, CH), F32) if g == 0 else halo_in[g - 1, w, :, 0:CH]
+            before = jnp.where(c == 1, halo_in[g, w, :, 0:CH], other)
+            one, two = before[7:8, :], before[6:7, :]
+            now = gated[w]
+            back1 = jnp.where(row == 0, one, pltpu.roll(now, 1, 0))
+            back2 = pltpu.roll(now, 2, 0)
+            back2 = jnp.where(row == 0, two, jnp.where(row == 1, one, back2))
+            conv = taps[w, 0:1, 0:CH] * back2 + taps[w, 1:2, 0:CH] * back1 + taps[w, 2:3, 0:CH] * now
+            mixed = outer[w] * conv
+            hid[g * ROWS:(g + 1) * ROWS, w * 256:(w + 1) * 256] = jnp.concatenate(
+                [jnp.zeros((ROWS, 12), F32), mixed, jnp.zeros((ROWS, 112), F32)], axis=1
+            ).astype(BF16)
+        rows = slice(g * ROWS, (g + 1) * ROWS)
+        scatter(1, g, lambda q: dot_t(hid[rows, 0:512], weights(q, [(mb, 0, 0, 256), (mb, 1, 0, 256)])))
+
+    def mixer_weights(count):
+        for _ in range(count):
+            if later:
+                slot_of(1, later.pop(0))
+
+    ffn(0, 0)
+    mixer_weights(1)
+    ffn(0, 1)
+    mixer_weights(1)
+    spread_rows(0, 0, 2, settle(0, 0, 1, 0.5))
+    mixer_weights(1)
+    spread_rows(0, 1, 2, settle(0, 1, 1, 0.5))
+    mixer_weights(10)
     complete(1)
-
-    gated, outer = [], []
-    project(((ma, 0, 0, 384), (mb, 0, 0, 256), (ma, 1, 0, 384), (mb, 1, 0, 256)), incoming)
-    for w in range(2):
-        both = jnp.concatenate([proj[2 * w], proj[2 * w + 1, :, 0:256]], axis=1).astype(BF16).astype(F32)
-        outer.append(both[:, 0:CH])
-        product = both[:, CH:2 * CH] * both[:, 2 * CH:3 * CH]
-        gated.append(product)
-        halo_out[w, :, 0:CH] = product[HALF - 8:HALF, :]
-    hcopy = pltpu.make_async_remote_copy(
-        src_ref=halo_out, dst_ref=halo_in, send_sem=h_send, recv_sem=h_recv,
-        device_id=mate, device_id_type=pl.DeviceIdType.MESH,
-    )
-    hcopy.start()
-    hcopy.wait()
-    row = lax.broadcasted_iota(jnp.int32, (HALF, CH), 0)
-    for w in range(2):
-        before = jnp.where(c == 1, halo_in[w, :, 0:CH], 0.0)
-        one, two = before[7:8, :], before[6:7, :]
-        g = gated[w]
-        back1 = jnp.where(row == 0, one, pltpu.roll(g, 1, 0))
-        back2 = pltpu.roll(g, 2, 0)
-        back2 = jnp.where(row == 0, two, jnp.where(row == 1, one, back2))
-        conv = taps[w, 0:1, 0:CH] * back2 + taps[w, 1:2, 0:CH] * back1 + taps[w, 2:3, 0:CH] * g
-        mixed = outer[w] * conv
-        hid[:, w * 256:(w + 1) * 256] = jnp.concatenate(
-            [jnp.zeros((HALF, 12), F32), mixed, jnp.zeros((HALF, 112), F32)], axis=1
-        ).astype(BF16)
-
-    def mixer_parts(q):
-        return dot_t(hid[:, 0:256], weight(mb, 0, q, 0, 256)) + dot_t(hid[:, 256:512], weight(mb, 1, q, 0, 256))
-
-    incoming = narrow(1, mixer_parts, 3, 1.0, False)
-    ffn(2, 5, True, incoming)
-
-    def mine_of(half, d):
-        return pl.ds(pl.multiple_of(half * HALF + lax.rem(x + NX - d, NX) * SHARE, SHARE), SHARE)
-
-    def result(index, rows, dev, sems):
+    mixer(0)
+    mixer(1)
+    spread_rows(1, 0, 4, settle(1, 0, 3, 1.0))
+    spread_rows(1, 1, 4, settle(1, 1, 3, 1.0))
+    ffn(2, 0)
+    ffn(2, 1)
+
+    outs, mate_outs, backs = [], [], []
+
+    def result(g, d, dev, sems):
+        rows = token_rows(g, c, lax.rem(x + NX - d, NX), SHARE)
         return pltpu.make_async_remote_copy(
-            src_ref=fin.at[rows, :], dst_ref=fin.at[rows, :], send_sem=sems[0].at[index], recv_sem=sems[1].at[index],
+            src_ref=fin.at[rows, :], dst_ref=fin.at[rows, :], send_sem=sems[0].at[g, d], recv_sem=sems[1].at[g, d],
             device_id=dev, device_id_type=pl.DeviceIdType.MESH,
         )
 
-    fin[mine_of(c, 0), :] = res[...]
-    outs, mate_outs = [], []
-    for d in (2, 1, 3):
-        outs.append(result(d, mine_of(c, 0), peers[d - 1], (fo_send, fo_recv)))
-        outs[-1].start()
-    for d in (0, 1, 3, 2):
-        if d > 0:
-            result(d, mine_of(c, d), mate, (fo_send, fo_recv)).wait_recv()
-        mate_outs.append(result(d, mine_of(c, d), mate, (fp_send, fp_recv)))
+    for g in range(GROUPS):
+        fin[token_rows(g, c, x, SHARE), :] = settle(2, g, 5, 0.5)
+        for d in (2, 1, 3):
+            outs.append(pltpu.make_async_remote_copy(
+                src_ref=fin.at[token_rows(g, c, x, SHARE), :], dst_ref=fin.at[token_rows(g, c, x, SHARE), :],
+                send_sem=fo_send.at[g, d], recv_sem=fo_recv.at[g, d],
+                device_id=peers[d - 1], device_id_type=pl.DeviceIdType.MESH,
+            ))
+            outs[-1].start()
+        mate_outs.append(result(g, 0, mate, (fp_send, fp_recv)))
         mate_outs[-1].start()
-    backs = []
-    for turn, h in enumerate((c, 1 - c)):
-        if turn == 1:
-            for copy in mate_outs:
-                copy.wait_recv()
-        tokens = pl.ds(pl.multiple_of(h * HALF, HALF), HALF)
+    for g in range(GROUPS):
+        for d in (1, 3, 2):
+            result(g, d, mate, (fo_send, fo_recv)).wait_recv()
+            mate_outs.append(result(g, d, mate, (fp_send, fp_recv)))
+            mate_outs[-1].start()
+        for d in range(NX):
+            result(g, d, mate, (fp_send, fp_recv)).wait_recv()
         acc[...] = jnp.zeros_like(acc)
         for j, base, width in windows():
-            acc[base:base + width, :] += dot_t(spread(j, base, width), fin[tokens, 384 * j:384 * (j + 1)])
-        fout[turn] = acc[...].astype(BF16)
-        backs.append(pltpu.make_async_copy(fout.at[turn], out.at[:, tokens], l_sem.at[turn]))
+            acc[base:base + width, :] += dot_t(spread(j, base, width), fin[g * HALF:(g + 1) * HALF, 384 * j:384 * (j + 1)])
+        fout[g] = acc[...].astype(BF16)
+        backs.append(pltpu.make_async_copy(fout.at[g], out.at[:, pl.ds(g * HALF, HALF)], l_sem.at[g]))
         backs[-1].start()
+    for copies in reduced.values():
+        for copy in copies:
+            copy.wait_send()
     for copy in started + [copy for _, copy in mates] + outs + mate_outs:
         copy.wait_send()
     for copy in backs:
@@ -424,26 +444,26 @@
             pltpu.VMEM((2, NZ, NY * PAD + 8, 256), BF16),
             pltpu.VMEM((HALF, DP), BF16),
             pltpu.VMEM((QN, HALF, QW), BF16),
-            pltpu.VMEM((4, HALF, HID), F32),
+            pltpu.VMEM((GROUPS, 2, ROWS, 2 * HID), F32),
             pltpu.VMEM((HALF, 2 * HID), BF16),
             pltpu.VMEM((3, QN, HALF, QW), BF16),
-            pltpu.VMEM((3, QN, SHARE, QW), BF16),
+            pltpu.VMEM((GROUPS, 3, QN, SHARE, QW), BF16),
             pltpu.VMEM((SHARE, DP), F32),
-            pltpu.VMEM((SHARE, DP), BF16),
+            pltpu.VMEM((GROUPS, SHARE, DP), BF16),
             pltpu.VMEM((2 * HALF, DP), BF16),
             pltpu.VMEM((D, HALF), F32),
             pltpu.VMEM((2, D, HALF), BF16),
             pltpu.VMEM((8, DP), F32),
             pltpu.VMEM((2, 8, 256), F32),
-            pltpu.VMEM((2, 8, 256), F32),
-            pltpu.VMEM((2, 8, 256), F32),
+            pltpu.VMEM((GROUPS, 2, 8, 256), F32),
+            pltpu.VMEM((GROUPS, 2, 8, 256), F32),
             dma((4, 96)), dma((4, 96)),
             dma((4, 12)), dma((4, 12)),
-            dma((3, 3, 3)), dma((3, 3, 3)),
-            dma((2, 3, 3)), dma((2, 3, 3)),
-            dma((4,)), dma((4,)),
-            dma((4,)), dma((4,)),
-            dma(()), dma(()),
+            dma((3, GROUPS, 3, 3)), dma((3, GROUPS, 3, 3)),
+            dma((2, GROUPS, 3, 3)), dma((2, GROUPS, 3, 3)),
+            dma((GROUPS, NX)), dma((GROUPS, NX)),
+            dma((GROUPS, NX)), dma((GROUPS, NX)),
+            dma((GROUPS,)), dma((GROUPS,)),
             dma((10,)),
         ],
         compiler_params=pltpu.CompilerParams(

time: 134 us -> 128 us (0.955)
  Pallas kernels: 132 us -> 126 us
    pallas_call x1, Pallas kernels: 132 us -> 126 us  [local(): pl.pallas_call(kernel, out_shape=jax.ShapeDtypeStruct((D, 2 * HALF), BF16...]
where the time goes in v3:
time: 128 us
  Pallas kernels  126 us (98%)
  local copies, waits for them, and re-layouts  2.29 us (2%)
    pallas_call x1, Pallas kernels, local(): pl.pallas_call(kernel, out_shape=jax.ShapeDtypeStruct((D, 2 * HALF), BF16...  126 us

profile of v3, /device:TPU:1, one launch (start us, length us, event | category | flops | bytes accessed | tf_op | source)
XLA Modules:
  0.0 127.9 jit_solution(11210063602298636937)
XLA Ops:
  0.0 125.6 %layer.1 = bf16[2112,256]{1,0:T(8,128)(2,1)} custom-call(bf16[22,384]{1,0:T(8,128)(2,1)} %gate_in.1, bf16[22,384]{1,0:T(8,128)(2,1)} %up_in.1, bf16[22,384]{1,0:T(8,128)(2,1)} %down_in.1, bf16[22,132]{1,0:T(8,128)(2,1)} %outer_in.1, bf16[22,132]{1,0:T(8,128)(2,1)} %inner_in.1, bf16[22,132]{1,0:T(8,128)(2,1)} %value_in.1, bf16[22,132]{1,0:T(8,128)(2,1)} %mixer_in.1, ...), custom_call_target="tpu_custom_call" | custom-call | tf_op jit(solution)/shard_map/layer/pallas_call | solution.py:432
  125.6 2.3 %copy.12 = bf16[256,2112]{0,1:T(8,128)(2,1)} copy(bf16[256,2112]{0,1:T(8,128)(2,1)} %bitcast.2) | data formatting | bytes 2162688

commit v4 on v3

--- a/solution.py
+++ b/solution.py
@@ -15,7 +15,8 @@
 GROUPS, HALF = 2, 128
 ROWS, SHARE = HALF // GROUPS, 16
 HID, CH = 384, 132
-LAG = 5
+SLOTS = 8
+FOLLOW = {2: (1,), 3: (2,), 7: (3,)}
 F32, BF16 = jnp.float32, jnp.bfloat16
 
 
@@ -46,7 +47,7 @@
 
 
 def kernel(
-    gate_in, up_in, down_in, outer_in, inner_in, value_in, mixer_in, stream_in, gains_in, taps_in, out,
+    gate_in, up_in, down_in, outer_in, inner_in, value_in, mixer_in, stream_in, gains_in, taps_in, out_a, out_b,
     gate_sh, up_sh, down_sh, outer_sh, inner_sh, value_sh, mixer_sh, stream, gains_raw, taps_raw,
     wa, wb, ma, mb, xs, xn, proj, hid, part, got, tot, res, fin, acc, fout, gains, taps, halo_out, halo_in,
     g_send, g_recv, p_send, p_recv, rs_send, rs_recv, ag_send, ag_recv,
@@ -61,10 +62,10 @@
         return {"fs": zz * NY + yy, "tp": xx * 2 + cc}
 
     def ymod(v):
-        return lax.rem(v + NY, NY)
+        return lax.rem(v + 2 * NY, NY)
 
     def zmod(v):
-        return lax.rem(v + NZ, NZ)
+        return lax.rem(v + 2 * NZ, NZ)
 
     arrivals = [
         pltpu.make_async_copy(src, dst, l_sem.at[i])
@@ -78,10 +79,12 @@
 
     y_fwd, y_back = at(z, ymod(y + s), x, c), at(z, ymod(y - s), x, c)
     z_fwd, z_back = at(zmod(z + s), y, x, c), at(zmod(z - s), y, x, c)
+    y_fwd2, y_back2 = at(z, ymod(y + 2 * s), x, c), at(z, ymod(y - 2 * s), x, c)
+    z_fwd2, z_back2 = at(zmod(z + 2 * s), y, x, c), at(zmod(z - 2 * s), y, x, c)
     mate = at(z, y, x, 1 - c)
     peers = [at(z, y, lax.rem(x + d, NX), c) for d in (1, 2, 3)]
     barrier = pltpu.get_barrier_semaphore()
-    for dev in [y_fwd, y_back, z_fwd, z_back, mate] + peers:
+    for dev in [y_fwd, y_back, z_fwd, z_back, y_fwd2, y_back2, z_fwd2, z_back2, mate] + peers:
         pl.semaphore_signal(barrier, inc=1, device_id=dev, device_id_type=pl.DeviceIdType.MESH)
     for copy in arrivals[:7]:
         copy.wait()
@@ -100,7 +103,7 @@
     ).astype(BF16)
     ma[c, z, here, :] = mix[:, 0:384]
     mb[c, z, here, :] = mix[:, 384:640]
-    pl.semaphore_wait(barrier, 8)
+    pl.semaphore_wait(barrier, 12)
 
     ys = [y] + [ymod(y - s * d) for d in range(1, 5)] + [ymod(y + s * d) for d in range(1, 4)]
     zs = [z] + [zmod(z - s * d) for d in range(1, 7)] + [zmod(z + s * d) for d in range(1, 6)]
@@ -123,22 +126,38 @@
     def take(which, jz, jy):
         remote(which, zs[jz], ys[jy], jz * NY + jy, y_fwd).wait_recv()
 
-    y_hops = ((0, 4, y_fwd), (4, 3, y_back))
-    z_hops = ((0, 6, z_fwd), (6, 5, z_back))
+    y_hops = ((0, 4, y_fwd, y_fwd2), (4, 3, y_back, y_back2))
+    z_hops = ((0, 6, z_fwd, z_fwd2), (6, 5, z_back, z_back2))
 
     def y_next(which, jz, jy):
-        for off, hops, dev in y_hops:
+        for off, hops, dev, _ in y_hops:
             if jy == 0:
                 push(which, jz, 0, jz, off + 1, dev)
             elif off < jy < off + hops:
                 push(which, jz, jy, jz, jy + 1, dev)
 
     def z_next(which, jz, jy):
-        for off, hops, dev in z_hops:
+        for off, hops, dev, _ in z_hops:
             if jz == 0:
                 push(which, 0, jy, off + 1, jy, dev)
             elif off < jz < off + hops:
                 push(which, jz, jy, jz + 1, jy, dev)
+
+    def leap(which, jz, jy):
+        along_z = which % 2 == 1
+        own = jz if along_z else jy
+        for off, hops, dev, dev2 in z_hops if along_z else y_hops:
+            if own == 0:
+                targets = ((off + 1, dev), (off + 2, dev2))
+            elif off < own <= off + hops - 2:
+                targets = ((own + 2, dev2),)
+            else:
+                targets = ()
+            for to, where in targets:
+                if along_z:
+                    push(which, jz, 0, to, 0, where)
+                else:
+                    push(which, 0, jy, 0, to, where)
 
     def y_far(jy):
         return jy if jy <= 4 else jy - 4
@@ -162,32 +181,33 @@
 
     def own_out(group):
         even, odd = 2 * group, 2 * group + 1
+        leap(odd, 0, 0)
+        leap(even, 0, 0)
         z_next(even, 0, 0)
         y_next(odd, 0, 0)
-        y_next(even, 0, 0)
-        z_next(odd, 0, 0)
 
     def slot_of(group, slot):
         even, odd = 2 * group, 2 * group + 1
         first = [(0, jy) for jy in y_order[1:]] + [(jz, jy) for jz in z_order[1:] for jy in y_order]
         second = [(jz, 0) for jz in z_order[1:]] + [(jz, jy) for jy in y_order[1:] for jz in z_order]
-        first, second = (
-            [(jz, jy) for jz, jy in blocks if z_far(jz) + y_far(jy) == slot] for blocks in (first, second)
-        )
+        first = [(jz, jy) for jz, jy in first if z_far(jz) + (y_far(jy) + 1) // 2 == slot]
+        second = [(jz, jy) for jz, jy in second if (z_far(jz) + 1) // 2 + y_far(jy) == slot]
         for i in range(max(len(first), len(second))):
             for which, blocks in ((even, first), (odd, second)):
                 if i < len(blocks):
                     jz, jy = blocks[i]
                     take(which, jz, jy)
-                    if which == even or jy == 0:
+                    if (jz if which == even else jy) == 0:
+                        leap(which, jz, jy)
+                    if which == even:
                         z_next(which, jz, jy)
-                    if which == odd or jz == 0:
+                    else:
                         y_next(which, jz, jy)
         for jz in range(NZ):
-            if slot == 4 + z_far(jz):
+            if slot == 2 + z_far(jz):
                 to_mate(even, None, jz)
         for jy in range(NY):
-            if slot == 6 + y_far(jy):
+            if slot == 3 + y_far(jy):
                 to_mate(odd, bufs[odd].at[c, :, pl.ds(pl.multiple_of(ys[jy] * PAD, 8), PAD), :], jy)
 
     def complete(group):
@@ -232,21 +252,20 @@
             taps[w, 0:3, :] = dot(taps_raw[...], pick)
 
     own_out(0)
+    own_out(1)
     for copy in arrivals[7:]:
         copy.wait()
-    for slot in range(1, 11):
+    for slot in range(1, SLOTS + 1):
         slot_of(0, slot)
-        if slot > LAG:
-            slot_of(1, slot - LAG)
-        if slot == LAG:
-            own_out(1)
+        for follower in FOLLOW.get(slot, ()):
+            slot_of(1, follower)
         if slot <= 6:
             window(*windows()[slot - 1])
         if slot == 7:
             first_norm()
         if slot == 8:
             own_taps()
-    later = list(range(11 - LAG, 11))
+    later = list(range(1 + max(slot for slots in FOLLOW.values() for slot in slots), SLOTS + 1))
     complete(0)
 
     def weights(q, pieces):
@@ -415,7 +434,7 @@
         for j, base, width in windows():
             acc[base:base + width, :] += dot_t(spread(j, base, width), fin[g * HALF:(g + 1) * HALF, 384 * j:384 * (j + 1)])
         fout[g] = acc[...].astype(BF16)
-        backs.append(pltpu.make_async_copy(fout.at[g], out.at[:, pl.ds(g * HALF, HALF)], l_sem.at[g]))
+        backs.append(pltpu.make_async_copy(fout.at[g], (out_a, out_b)[g], l_sem.at[g]))
         backs[-1].start()
     for copies in reduced.values():
         for copy in copies:
@@ -429,11 +448,11 @@
 def local(stream_in, norm_gains, gate_proj, up_proj, down_proj, outer_gate, inner_gate, value_proj, mixer_out, conv_taps):
     hbm = pl.BlockSpec(memory_space=pl.ANY)
     dma = pltpu.SemaphoreType.DMA
-    return pl.pallas_call(
+    halves = pl.pallas_call(
         kernel,
-        out_shape=jax.ShapeDtypeStruct((D, 2 * HALF), BF16),
+        out_shape=[jax.ShapeDtypeStruct((D, HALF), BF16)] * GROUPS,
         in_specs=[hbm] * 10,
-        out_specs=hbm,
+        out_specs=[hbm] * GROUPS,
         scratch_shapes=[
             pltpu.VMEM((OWN, HID), BF16), pltpu.VMEM((OWN, HID), BF16), pltpu.VMEM((OWN, HID), BF16),
             pltpu.VMEM((OWN, CH), BF16), pltpu.VMEM((OWN, CH), BF16), pltpu.VMEM((OWN, CH), BF16), pltpu.VMEM((OWN, CH), BF16),
@@ -470,7 +489,8 @@
             collective_id=0, has_side_effects=True, vmem_limit_bytes=58 * 1024 * 1024
         ),
         name="layer",
-    )(gate_proj, up_proj, down_proj, outer_gate, inner_gate, value_proj, mixer_out, stream_in.T, norm_gains, conv_taps).T
+    )(gate_proj, up_proj, down_proj, outer_gate, inner_gate, value_proj, mixer_out, stream_in.T, norm_gains, conv_taps)
+    return jnp.concatenate(halves, axis=1).T
 
 
 def solution(mesh):

time: 128 us -> 127 us (level)
  other arithmetic: 0 us -> 2.31 us
  local copies, waits for them, and re-layouts: 2.29 us -> 0 us
    transpose x0 -> x1, other arithmetic: none -> 2.31 us  [local(): return jnp.concatenate(halves, axis=1).T]
    unnamed x1 -> x0, local copies, waits for them, and re-layouts: 2.29 us -> none
where the time goes in v4:
time: 127 us
  Pallas kernels  125 us (98%)
  other arithmetic  2.31 us (2%)
    pallas_call x1, Pallas kernels, local(): pl.pallas_call(kernel, out_shape=[jax.ShapeDtypeStruct((D, HALF), BF16)]...  125 us

profile of v4, /device:TPU:1, one launch (start us, length us, event | category | flops | bytes accessed | tf_op | source)
XLA Modules:
  0.0 127.3 jit_solution(6597391064199565145)
XLA Ops:
  0.0 125.0 %layer.1 = (bf16[2112,128]{1,0:T(8,128)(2,1)}, bf16[2112,128]{1,0:T(8,128)(2,1)}) custom-call(bf16[22,384]{1,0:T(8,128)(2,1)} %gate_in.1, bf16[22,384]{1,0:T(8,128)(2,1)} %up_in.1, bf16[22,384]{1,0:T(8,128)(2,1)} %down_in.1, bf16[22,132]{1,0:T(8,128)(2,1)} %outer_in.1, bf16[22,132]{1,0:T(8,128)(2,1)} %inner_in.1, bf16[22,132]{1,0:T(8,128)(2,1)} %value_in.1, ...), custom_call_target="tpu_custom_call" | custom-call | tf_op jit(solution)/shard_map/layer/pallas_call | solution.py:451
  125.0 2.3 %maximum_bitcast_fusion = bf16[256,2112]{0,1:T(8,128)(2,1)} fusion(bf16[2112,128]{1,0:T(8,128)(2,1)} %get-tuple-element.8, bf16[2112,128]{1,0:T(8,128)(2,1)} %get-tuple-element.7), kind=kLoop, calls=%fused_computation | loop fusion | flops 2162688 | bytes 2162688 | tf_op jit(solution)/shard_map/transpose | solution.py:493
